TPU v7x, 1024 devices: a 2x16x16 block of a 4x16x16 slice. The times are simulated.
1024 devices in a mesh: grp: 2 (over x), tp: 16 (over z), dp: 32 (over y, core).
Axes of the slice: x: 2, y: 16, z: 16, core: 2. Of those that a mesh axis runs over, the one named last changes fastest.
The devices are a block of a 4x16x16 slice.
Arguments:
- tokens: bfloat16 [256, 4096], P(('grp', 'tp'), 'dp'), parts along dimension 0, may hold values from -30 to 30
- norm_gain: float32 [2, 4096], P(None, 'dp'), may hold values from 0.1 to 1.9
- w_query: bfloat16 [2, 4096, 2048], P(None, 'dp', 'tp'), may hold values from -0.09375 to 0.09375
- w_forget: bfloat16 [2, 4096, 2048], P(None, 'dp', 'tp'), may hold values from -0.09375 to 0.09375
- w_value: bfloat16 [2, 4096, 2048], P(None, 'dp', 'tp'), may hold values from -0.09375 to 0.09375
- w_gate: bfloat16 [2, 4096, 2048], P(None, 'dp', 'tp'), may hold values from -0.09375 to 0.09375
- lower_bound: float32 [2, 2048], P(None, 'tp'), may hold values from 0 to 0.9
- head_gain: float32 [2, 128], replicated, may hold values from 0.1 to 1.9
- w_out: bfloat16 [2, 2048, 4096], P(None, 'tp', 'dp'), may hold values from -0.125 to 0.125
- state: float32 [2, 256, 16, 128, 128], P(None, ('grp', 'dp'), 'tp'), parts along dimension 1, may hold values from -4 to 4
Outputs:
- hidden_out: bfloat16 [256, 4096], P(('grp', 'tp'), 'dp'), parts along dimension 0
- new_state: float32 [2, 256, 16, 128, 128], P(None, ('grp', 'dp'), 'tp'), parts along dimension 1
There are 2 independent parts, one for each index of `grp`. A program takes and returns all parts, laid end to end along the dimension named above; an argument that names none is the same for every part. Nothing has to cross between parts.
All inputs are finite; a program needn't handle non-finite values.
Results may differ from a plain program's by a relative error of at most 0.02.
Values may be sent and summed in bfloat16 or wider, within the bound.
No kernel may reach another device: no remote copies, remote signals or barrier semaphores. Data moves between devices by JAX's collectives and lax.ppermute only.
A program may use at most 32 MiB of HBM per device.

v0:
```python
import math

import jax
import jax.numpy as jnp
from jax import lax
from jax.sharding import PartitionSpec as P

D = 4096
HD = 128


def sent_to_all(x, axis):
    length = lax.axis_size(axis)
    return lax.all_to_all(jnp.broadcast_to(x[None], (length, *x.shape)), axis, 0, 0, tiled=True)


def joined_along(parts, dim):
    parts = jnp.moveaxis(parts, 0, dim)
    shape = parts.shape
    return parts.reshape(*shape[:dim], shape[dim] * shape[dim + 1], *shape[dim + 2 :])


def gather_directly(x, axis, dim):
    parts = sent_to_all(x, axis)
    return joined_along(parts, dim)


def in_blocks(x, dim, length):
    before, after = (x.shape[:dim], x.shape[dim + 1 :])
    return jnp.moveaxis(x.reshape(*before, length, -1, *after), dim, 0)


def summed_on_arrival(x, axis, dim):
    parts = in_blocks(x, dim, lax.axis_size(axis))
    arrived = lax.all_to_all(parts, axis, split_axis=0, concat_axis=0, tiled=True)
    return arrived.astype(jnp.float32).sum(axis=0)


def in_one_piece(arrays, axis, dim, along):
    widths = [math.prod(a.shape[along:]) for a in arrays]
    both = jnp.concatenate(
        [a.reshape(*a.shape[:along], w) for a, w in zip(arrays, widths)], axis=along
    )
    out = summed_on_arrival(both, axis, dim)
    parts = jnp.split(out, [sum(widths[:k]) for k in range(1, len(widths))], axis=along)
    return tuple((b.reshape(*out.shape[:along], *a.shape[along:]) for a, b in zip(arrays, parts)))


def per_device(
    tokens, norm_gain, w_query, w_forget, w_value, w_gate, lower_bound, head_gain, w_out, state
):
    local_seqs = state.shape[1]
    head_count = state.shape[2]
    hidden = tokens
    updated = []
    for layer in range(2):
        gathered = gather_directly(hidden, "tp", 0)
        widened = gathered.astype(jnp.float32)
        squares = jnp.sum(widened * widened, axis=1)
        scaled = (widened * norm_gain[layer]).astype(jnp.bfloat16)
        joined = jnp.concatenate(
            [
                jnp.dot(scaled, weight[layer], preferred_element_type=jnp.float32)
                for weight in (w_query, w_forget, w_value, w_gate)
            ],
            axis=1,
        )
        payload = (joined, squares)
        shares = in_one_piece(
            (payload[0].astype(jnp.bfloat16), payload[1].astype(jnp.bfloat16)), "dp", 0, 1
        )
        own_squares = shares[1]
        own_proj = shares[0]
        width = own_proj.shape[1] // 4
        factor = lax.rsqrt(own_squares / D + 1e-06)[:, None]
        query, forget_pre, value, gate_pre = (
            own_proj[:, index * width : (index + 1) * width] * factor for index in range(4)
        )
        bound = lower_bound[layer]
        forget = bound + (1.0 - bound) * jax.nn.sigmoid(forget_pre)
        keyvec = (1.0 - bound) * jax.nn.sigmoid(-forget_pre)

        def shaped(array):
            return array.reshape(local_seqs, head_count, HD)

        carried = (
            shaped(forget)[..., None] * state[layer]
            + shaped(keyvec)[..., None] * shaped(value)[..., None, :]
        )
        updated.append(carried)
        readout = jnp.einsum("bhkv,bhk->bhv", carried, shaped(query))
        readout = (
            readout
            * lax.rsqrt(jnp.mean(readout * readout, axis=-1, keepdims=True) + 1e-06)
            * head_gain[layer]
        )
        normed = (readout.reshape(local_seqs, head_count * HD) * jax.nn.sigmoid(gate_pre)).astype(
            jnp.bfloat16
        )
        out_weight = w_out[layer]
        mixed = jnp.dot(
            gather_directly(normed, "dp", 0), out_weight, preferred_element_type=jnp.float32
        )
        mixed_sum = summed_on_arrival(mixed.astype(jnp.bfloat16), "tp", 0)
        hidden = (hidden.astype(jnp.float32) + mixed_sum).astype(jnp.bfloat16)
    return (hidden, jnp.stack(updated))


def solution(mesh):
    return jax.shard_map(
        per_device,
        mesh=mesh,
        in_specs=(
            P(("grp", "tp"), "dp"),
            P(None, "dp"),
            P(None, "dp", "tp"),
            P(None, "dp", "tp"),
            P(None, "dp", "tp"),
            P(None, "dp", "tp"),
            P(None, "tp"),
            P(),
            P(None, "tp", "dp"),
            P(None, ("grp", "dp"), "tp", None, None),
        ),
        out_specs=(P(("grp", "tp"), "dp"), P(None, ("grp", "dp"), "tp", None, None)),
        check_vma=False,
    )
```

profile of v0, /device:TPU:5, one launch (start us, length us, event | category | flops | bytes accessed | tf_op | source)
XLA Modules:
  0.0 240.9 jit_solution(7161814434998576468)
XLA Ops:
  0.6 1.3 broadcast_in_dim.8
  1.9 83.8 %all-to-all-start = ((bf16[16,8,128]{2,1,0:T(8,128)(2,1)}), bf16[16,8,128]{2,1,0:T(8,128)(2,1)S(1)}, u32[]{:S(2)}, u32[]{:S(2)}) async-start(bf16[16,8,128]{2,1,0:T(8,128)(2,1)} %broadcast_in_dim.8), calls=%async_computation | async-start | bytes 65536 | tf_op jit(solution)/shard_map/all_to_all | solution.py:14
  85.7 11.2 %all-to-all-done = bf16[16,8,128]{2,1,0:T(8,128)(2,1)S(1)} async-done(((bf16[16,8,128]{2,1,0:T(8,128)(2,1)}), bf16[16,8,128]{2,1,0:T(8,128)(2,1)S(1)}, u32[]{:S(2)}, u32[]{:S(2)}) %all-to-all-start) | async-done | bytes 32800 | tf_op jit(solution)/shard_map/all_to_all | solution.py:14
  97.2 0.4 copy.84
  97.7 0.7 copy-done.1
  98.4 0.1 fusion.6
  98.5 0.7 copy-done.2
  99.3 0.7 copy-done.3
  100.2 0.8 copy.85
  101.0 16.6 %all-to-all-start.1 = ((bf16[32,4,513]{2,1,0:T(4,128)(2,1)}), bf16[32,4,513]{2,1,0:T(4,128)(2,1)S(1)}, u32[]{:S(2)}, u32[]{:S(2)}) async-start(bf16[32,4,513]{2,1,0:T(4,128)(2,1)} %copy.85), calls=%async_computation.1 | async-start | bytes 327680 | tf_op jit(solution)/shard_map/all_to_all | solution.py:35
  117.6 0.7 copy-done.6
  118.2 16.3 %all-to-all-done.1 = bf16[32,4,513]{2,1,0:T(4,128)(2,1)S(1)} async-done(((bf16[32,4,513]{2,1,0:T(4,128)(2,1)}), bf16[32,4,513]{2,1,0:T(4,128)(2,1)S(1)}, u32[]{:S(2)}, u32[]{:S(2)}) %all-to-all-start.1) | async-done | bytes 131360 | tf_op jit(solution)/shard_map/all_to_all | solution.py:35
  134.8 0.3 fusion.14
  135.4 16.6 %all_to_all.40 = bf16[32,4,128]{2,1,0:T(4,128)(2,1)S(1)} all-to-all(bf16[32,4,128]{2,1,0:T(4,128)(2,1)S(1)} %broadcast_in_dim.9), channel_id=1, replica_groups=mesh['grp'=2,'tp'=16,'dp'=32] {'dp'}, dimensions={0} | all-to-all | bytes 65536 | tf_op jit(solution)/shard_map/all_to_all | solution.py:14
  152.1 13.9 %all_to_all.41 = bf16[16,8,128]{2,1,0:T(8,128)(2,1)S(1)} all-to-all(bf16[16,8,128]{2,1,0:T(8,128)(2,1)S(1)} %fusion.8), channel_id=1, replica_groups=mesh['grp'=2,'tp'=16,'dp'=32] {'tp'}, dimensions={0} | all-to-all | bytes 65536 | tf_op jit(solution)/shard_map/all_to_all | solution.py:35
  166.1 0.7 copy-done.5
  166.7 13.9 %all_to_all.42 = bf16[16,8,128]{2,1,0:T(8,128)(2,1)S(1)} all-to-all(bf16[16,8,128]{2,1,0:T(8,128)(2,1)S(1)} %broadcast_in_dim.10), channel_id=1, replica_groups=mesh['grp'=2,'tp'=16,'dp'=32] {'tp'}, dimensions={0} | all-to-all | bytes 65536 | tf_op jit(solution)/shard_map/all_to_all | solution.py:14
  180.9 0.4 copy.91
  181.4 0.2 fusion.2
  181.5 0.1 fusion.1
  181.7 0.1 fusion
  181.9 23.9 %all_to_all.43 = bf16[32,4,513]{2,1,0:T(4,128)(2,1)S(1)} all-to-all(bf16[32,4,513]{2,1,0:T(4,128)(2,1)S(1)} %copy.92), channel_id=1, replica_groups=mesh['grp'=2,'tp'=16,'dp'=32] {'dp'}, dimensions={0} | all-to-all | bytes 262656 | tf_op jit(solution)/shard_map/all_to_all | solution.py:35
  206.0 0.3 fusion.11
  206.6 0.6 broadcast_in_dim.11
  207.2 5.3 %all-to-all-start.6 = ((bf16[32,4,128]{2,1,0:T(4,128)(2,1)}), bf16[32,4,128]{2,1,0:T(4,128)(2,1)S(1)}, u32[]{:S(2)}, u32[]{:S(2)}) async-start(bf16[32,4,128]{2,1,0:T(4,128)(2,1)} %broadcast_in_dim.11), calls=%async_computation.6 | async-start | bytes 65536 | tf_op jit(solution)/shard_map/all_to_all | solution.py:14
  212.5 0.3 multiply_add_fusion.1
  212.9 11.8 %all-to-all-done.6 = bf16[32,4,128]{2,1,0:T(4,128)(2,1)S(1)} async-done(((bf16[32,4,128]{2,1,0:T(4,128)(2,1)}), bf16[32,4,128]{2,1,0:T(4,128)(2,1)S(1)}, u32[]{:S(2)}, u32[]{:S(2)}) %all-to-all-start.6) | async-done | bytes 32800 | tf_op jit(solution)/shard_map/all_to_all | solution.py:14
  224.7 0.7 fusion.9
  225.4 3.9 %all-to-all-start.7 = ((bf16[16,8,128]{2,1,0:T(8,128)(2,1)}), bf16[16,8,128]{2,1,0:T(8,128)(2,1)S(1)}, u32[]{:S(2)}, u32[]{:S(2)}) async-start(bf16[16,8,128]{2,1,0:T(8,128)(2,1)} %fusion.9), calls=%async_computation.7 | async-start | bytes 65536 | tf_op jit(solution)/shard_map/all_to_all | solution.py:35
  229.4 0.8 pad_maximum_fusion
  230.2 10.1 %all-to-all-done.7 = bf16[16,8,128]{2,1,0:T(8,128)(2,1)S(1)} async-done(((bf16[16,8,128]{2,1,0:T(8,128)(2,1)}), bf16[16,8,128]{2,1,0:T(8,128)(2,1)S(1)}, u32[]{:S(2)}, u32[]{:S(2)}) %all-to-all-start.7) | async-done | bytes 32800 | tf_op jit(solution)/shard_map/all_to_all | solution.py:35
  240.3 0.6 add_convert_fusion
  (47 shorter events, 2.2 us)
Async XLA Ops:
  1.9 83.8 %copy-start.7 = (f32[2,128]{1,0:T(2,128)S(1)}, f32[2,128]{1,0:T(2,128)}, u32[]{:S(2)}) copy-start(f32[2,128]{1,0:T(2,128)} %param.11) | copy-start | bytes 3076
  1.9 95.0 %all-to-all-start = ((bf16[16,8,128]{2,1,0:T(8,128)(2,1)}), bf16[16,8,128]{2,1,0:T(8,128)(2,1)S(1)}, u32[]{:S(2)}, u32[]{:S(2)}) async-start(bf16[16,8,128]{2,1,0:T(8,128)(2,1)} %broadcast_in_dim.8), calls=%async_computation | async-start | bytes 65536 | tf_op jit(solution)/shard_map/all_to_all | solution.py:14
  85.7 11.8 %copy-start.9 = (bf16[2,128,128]{2,1,0:T(8,128)(2,1)S(1)}, bf16[2,128,128]{2,1,0:T(8,128)(2,1)}, u32[]{:S(2)}) copy-start(bf16[2,128,128]{2,1,0:T(8,128)(2,1)} %param.12) | copy-start | bytes 196612
  97.5 0.8 copy-start.1
  98.4 0.8 copy-start.2
  99.2 0.8 copy-start.3
  100.0 34.8 %copy-start = (f32[2,4,1,128,128]{4,3,2,1,0:T(8,128)S(1)}, f32[2,4,1,128,128]{4,3,2,1,0:T(8,128)}, u32[]{:S(2)}) copy-start(f32[2,4,1,128,128]{4,3,2,1,0:T(8,128)} %param.19) | copy-start | bytes 1572868
  101.0 16.6 %copy-start.8 = (f32[2,128]{1,0:T(2,128)S(1)}, f32[2,128]{1,0:T(2,128)}, u32[]{:S(2)}) copy-start(f32[2,128]{1,0:T(2,128)} %param.17) | copy-start | bytes 3076
  101.0 33.6 %all-to-all-start.1 = ((bf16[32,4,513]{2,1,0:T(4,128)(2,1)}), bf16[32,4,513]{2,1,0:T(4,128)(2,1)S(1)}, u32[]{:S(2)}, u32[]{:S(2)}) async-start(bf16[32,4,513]{2,1,0:T(4,128)(2,1)} %copy.85), calls=%async_computation.1 | async-start | bytes 327680 | tf_op jit(solution)/shard_map/all_to_all | solution.py:35
  117.6 0.7 copy-start.6
  135.1 16.9 %copy-start.4 = (bf16[2,128,128]{2,1,0:T(8,128)(2,1)S(1)}, bf16[2,128,128]{2,1,0:T(8,128)(2,1)}, u32[]{:S(2)}) copy-start(bf16[2,128,128]{2,1,0:T(8,128)(2,1)} %param.18) | copy-start | bytes 196612
  166.0 0.7 copy-start.5
  207.2 17.4 %all-to-all-start.6 = ((bf16[32,4,128]{2,1,0:T(4,128)(2,1)}), bf16[32,4,128]{2,1,0:T(4,128)(2,1)S(1)}, u32[]{:S(2)}, u32[]{:S(2)}) async-start(bf16[32,4,128]{2,1,0:T(4,128)(2,1)} %broadcast_in_dim.11), calls=%async_computation.6 | async-start | bytes 65536 | tf_op jit(solution)/shard_map/all_to_all | solution.py:14
  225.4 14.8 %all-to-all-start.7 = ((bf16[16,8,128]{2,1,0:T(8,128)(2,1)}), bf16[16,8,128]{2,1,0:T(8,128)(2,1)S(1)}, u32[]{:S(2)}, u32[]{:S(2)}) async-start(bf16[16,8,128]{2,1,0:T(8,128)(2,1)} %fusion.9), calls=%async_computation.7 | async-start | bytes 65536 | tf_op jit(solution)/shard_map/all_to_all | solution.py:35
where the time goes:
time: 243 us; the launch traced here: 241 us
  starting transfers between devices  110 us (45%)
  blocking collectives  68.3 us (28%)
  waiting for transfers between devices  49.4 us (20%)
  local copies, waits for them, and re-layouts  7.16 us (3%)
  other arithmetic  2.9 us (1%)
  matrix products  2.63 us (1%)
    all_to_all x2, starting transfers between devices, sent_to_all(): lax.all_to_all(jnp.broadcast_to(x[None], (length, *x.shape)), axis, 0, 0,...  89.1 us
    all_to_all x2, blocking collectives, summed_on_arrival(): lax.all_to_all(parts, axis, split_axis=0, concat_axis=0, tiled=True)  37.8 us
    all_to_all x2, blocking collectives, sent_to_all(): lax.all_to_all(jnp.broadcast_to(x[None], (length, *x.shape)), axis, 0, 0,...  30.5 us
    all_to_all x2, waiting for transfers between devices, summed_on_arrival(): lax.all_to_all(parts, axis, split_axis=0, concat_axis=0, tiled=True)  26.4 us
    all_to_all x2, waiting for transfers between devices, sent_to_all(): lax.all_to_all(jnp.broadcast_to(x[None], (length, *x.shape)), axis, 0, 0,...  23 us
    all_to_all x2, starting transfers between devices, summed_on_arrival(): lax.all_to_all(parts, axis, split_axis=0, concat_axis=0, tiled=True)  20.5 us
  transfers between devices with their start and end apart: 4, of which 4 were waited for; matrix products, arithmetic and copies ran while one was open for 0% of the time, Pallas kernels for 0%

commit v1 on v0

v1 whole, which is shorter than its diff:
```python
import jax
import jax.numpy as jnp
from jax import lax
from jax.sharding import Mesh, PartitionSpec as P

D = 4096
HD = 128
NEAR = 4
BF16 = jnp.bfloat16
F32 = jnp.float32


def exchange(x, axis, groups=None):
    return lax.all_to_all(x, axis, 0, 0, tiled=True, axis_index_groups=groups)


def dot(a, b):
    return jnp.dot(a, b, preferred_element_type=F32)


def per_device(
    tokens, norm_gain, w_query, w_forget, w_value, w_gate, lower_bound, head_gain, w_out, state
):
    rows, width = tokens.shape
    local_seqs, head_count = state.shape[1:3]
    tp_size, y_size, c_size = (lax.axis_size(a) for a in ("tp", "y", "c"))
    assert c_size == 2 and rows == c_size * local_seqs and tp_size == y_size
    tp, core = lax.axis_index("tp"), lax.axis_index("c")
    held = y_size * local_seqs

    sent = jnp.broadcast_to(
        tokens.reshape(1, c_size, local_seqs, width), (tp_size, c_size, local_seqs, width)
    )
    got = exchange(sent.reshape(tp_size * c_size, local_seqs, width), ("tp", "c"))
    got = got.reshape(tp_size, c_size, local_seqs, width)
    own = jnp.where(core == 0, got[:, 0], got[:, 1]).reshape(held, width)
    mate = jnp.where(core == 0, got[:, 1], got[:, 0]).reshape(held, width)

    joined = jnp.concatenate([w_query, w_forget, w_value, w_gate], axis=2)
    joined = (joined.astype(F32) * norm_gain[:, :, None]).astype(BF16)
    packed = jnp.concatenate([joined, w_out], axis=2)
    other = lax.ppermute(packed, "c", [(0, 1), (1, 0)])
    proj_width = joined.shape[2]

    updated = []
    for layer in range(2):
        own_f, mate_f = own.astype(F32), mate.astype(F32)
        squares = jnp.sum(own_f * own_f + mate_f * mate_f, axis=1, keepdims=True)
        partial = dot(own, packed[layer, :, :proj_width]) + dot(mate, other[layer, :, :proj_width])
        payload = jnp.concatenate([partial.astype(BF16), squares.astype(BF16)], axis=1)
        got = exchange(payload.reshape(y_size, local_seqs, proj_width + 1), "y")
        total = jnp.sum(got.astype(F32), axis=0)
        factor = lax.rsqrt(total[:, proj_width:] / D + 1e-06)
        head_width = proj_width // 4
        query, forget_pre, value, gate_pre = (
            total[:, k * head_width : (k + 1) * head_width] * factor for k in range(4)
        )
        bound = lower_bound[layer]
        forget = bound + (1.0 - bound) * jax.nn.sigmoid(forget_pre)
        keyvec = (1.0 - bound) * jax.nn.sigmoid(-forget_pre)

        def shaped(array):
            return array.reshape(local_seqs, head_count, HD)

        carried = (
            shaped(forget)[..., None] * state[layer]
            + shaped(keyvec)[..., None] * shaped(value)[..., None, :]
        )
        updated.append(carried)
        readout = jnp.einsum("bhkv,bhk->bhv", carried, shaped(query))
        readout = (
            readout
            * lax.rsqrt(jnp.mean(readout * readout, axis=-1, keepdims=True) + 1e-06)
            * head_gain[layer]
        )
        normed = (readout.reshape(local_seqs, head_count * HD) * jax.nn.sigmoid(gate_pre)).astype(
            BF16
        )
        got = exchange(jnp.broadcast_to(normed[None], (y_size, *normed.shape)), "y")
        gathered = got.reshape(held, head_count * HD)
        mixed_own = dot(gathered, packed[layer, :, proj_width:])
        mixed_mate = dot(gathered, other[layer, :, proj_width:])
        if layer == 0:
            near = min(NEAR, tp_size)
            groups = [[j * near + i for i in range(near)] for j in range(tp_size // near)]
            mixed = jnp.concatenate([mixed_own, mixed_mate], axis=1).astype(BF16)
            got = exchange(mixed.reshape(near, held // near, 2 * width), "tp", groups)
            piece = jnp.sum(got.astype(F32), axis=0).astype(BF16)
            got = exchange(jnp.broadcast_to(piece[None], (tp_size, *piece.shape)), "tp")
            got = got.reshape(tp_size // near, near, held // near, 2 * width)
            mixed = jnp.sum(got.astype(F32), axis=0).reshape(held, 2 * width)
            own = (own_f + mixed[:, :width]).astype(BF16)
            mate = (mate_f + mixed[:, width:]).astype(BF16)
        else:
            mine = (jnp.arange(held) // local_seqs == tp)[:, None]
            mixed_own = (mixed_own + jnp.where(mine, own_f, 0.0)).astype(BF16)
            mixed_mate = (mixed_mate + jnp.where(mine, mate_f, 0.0)).astype(BF16)
            first = jnp.where(core == 0, mixed_own, mixed_mate)
            second = jnp.where(core == 0, mixed_mate, mixed_own)
            sent = jnp.stack(
                [a.reshape(tp_size, local_seqs, width) for a in (first, second)], axis=1
            )
            got = exchange(sent.reshape(tp_size * c_size, local_seqs, width), ("tp", "c"))
            got = got.reshape(tp_size, rows, width)
            hidden = jnp.sum(got.astype(F32), axis=0).astype(BF16)
    return (hidden, jnp.stack(updated))


def solution(mesh):
    grp, tp, dp = mesh.devices.shape
    fine = Mesh(mesh.devices.reshape(grp, tp, dp // 2, 2), ("grp", "tp", "y", "c"))
    dps = ("y", "c")
    weight = P(None, dps, "tp")
    held = P(None, ("grp", *dps), "tp", None, None)
    return jax.shard_map(
        per_device,
        mesh=fine,
        in_specs=(
            P(("grp", "tp"), dps),
            P(None, dps),
            weight,
            weight,
            weight,
            weight,
            P(None, "tp"),
            P(),
            P(None, "tp", dps),
            held,
        ),
        out_specs=(P(("grp", "tp"), dps), held),
        check_vma=False,
    )
```

time: 243 us -> 224 us (0.922)
  blocking collectives: 68.3 us -> 38.1 us
  starting transfers between devices: 110 us -> 121 us
  local copies, waits for them, and re-layouts: 7.16 us -> 3.77 us
  other arithmetic: 2.9 us -> 5.45 us
  waiting for transfers between devices: 49.4 us -> 51.9 us
    all_to_all x4 -> x3, blocking collectives: 68.3 us -> 38.1 us  [exchange(): return lax.all_to_all(x, axis, 0, 0, tiled=True, axis_index_groups=groups)]
    all_to_all x4 -> x5, starting transfers between devices: 110 us -> 118 us  [exchange(): return lax.all_to_all(x, axis, 0, 0, tiled=True, axis_index_groups=groups)]
    ppermute x0 -> x1, starting transfers between devices: none -> 2.97 us  [per_device(): other = lax.ppermute(packed, 'c', [(0, 1), (1, 0)])]
    unnamed x20 -> x12, local copies, waits for them, and re-layouts: 3.43 us -> 0.69 us
    all_to_all x4 -> x5, waiting for transfers between devices: 49.4 us -> 51.9 us  [exchange(): return lax.all_to_all(x, axis, 0, 0, tiled=True, axis_index_groups=groups)]
  transfers between devices with their start and end apart: 4 -> 6, of which waited for: 4 -> 5; matrix products, arithmetic and copies ran while one was open for 0% -> 1% of each run, Pallas kernels for 0% -> 0%
where the time goes in v1:
time: 224 us; the launch traced here: 223 us
  starting transfers between devices  121 us (54%)
  waiting for transfers between devices  51.9 us (23%)
  blocking collectives  38.1 us (17%)
  other arithmetic  5.45 us (2%)
  local copies, waits for them, and re-layouts  3.77 us (2%)
    all_to_all x5, starting transfers between devices, exchange(): return lax.all_to_all(x, axis, 0, 0, tiled=True, axis_index_groups=groups)  118 us
    all_to_all x5, waiting for transfers between devices, exchange(): return lax.all_to_all(x, axis, 0, 0, tiled=True, axis_index_groups=groups)  51.9 us
    all_to_all x3, blocking collectives, exchange(): return lax.all_to_all(x, axis, 0, 0, tiled=True, axis_index_groups=groups)  38.1 us
  transfers between devices with their start and end apart: 6, of which 5 were waited for; matrix products, arithmetic and copies ran while one was open for 1% of the time, Pallas kernels for 0%

profile of v1, /device:TPU:5, one launch (start us, length us, event | category | flops | bytes accessed | tf_op | source)
XLA Modules:
  0.0 223.2 jit_solution(2398596502262798359)
XLA Ops:
  0.6 1.3 broadcast_in_dim.23
  2.0 87.3 %all-to-all-start = ((bf16[32,4,128]{2,1,0:T(4,128)(2,1)}), bf16[32,4,128]{2,1,0:T(4,128)(2,1)S(1)}, u32[]{:S(2)}, u32[]{:S(2)}) async-start(bf16[32,4,128]{2,1,0:T(4,128)(2,1)} %bitcast.3), calls=%async_computation | async-start | bytes 65536 | tf_op jit(solution)/shard_map/all_to_all | solution.py:14
  89.4 1.0 multiply_convert_fusion
  90.5 3.0 %collective-permute-start = (bf16[2,128,640]{2,1,0:T(8,128)(2,1)S(1)}, bf16[2,128,640]{2,1,0:T(8,128)(2,1)S(1)}, u32[]{:S(2)}, u32[]{:S(2)}) collective-permute-start(bf16[2,128,640]{2,1,0:T(8,128)(2,1)S(1)} %pad_maximum_fusion.1), channel_id=1, source_target_pairs={{0,1},{1,0},{2,3},{3,2},{4,5},{5,4},{6,7},{7,6},{8,9},{9,8},{10,11... | collective-permute-start | bytes 983048 | tf_op jit(solution)/shard_map/ppermute | solution.py:42
  93.4 8.0 %all-to-all-done = bf16[32,4,128]{2,1,0:T(4,128)(2,1)S(1)} async-done(((bf16[32,4,128]{2,1,0:T(4,128)(2,1)}), bf16[32,4,128]{2,1,0:T(4,128)(2,1)S(1)}, u32[]{:S(2)}, u32[]{:S(2)}) %all-to-all-start) | async-done | bytes 32800 | tf_op jit(solution)/shard_map/all_to_all | solution.py:14
  101.8 0.1 fusion.15
  102.0 0.1 fusion
  102.1 0.7 pad_maximum_fusion.2
  102.8 11.3 %all-to-all-start.1 = ((bf16[16,4,513]{2,1,0:T(4,128)(2,1)}), bf16[16,4,513]{2,1,0:T(4,128)(2,1)S(1)}, u32[]{:S(2)}, u32[]{:S(2)}) async-start(bf16[16,4,513]{2,1,0:T(4,128)(2,1)} %pad_maximum_fusion.2), calls=%async_computation.1 | async-start | bytes 163840 | tf_op jit(solution)/shard_map/all_to_all | solution.py:14
  114.1 0.7 copy-done.4
  114.8 11.0 %all-to-all-done.1 = bf16[16,4,513]{2,1,0:T(4,128)(2,1)S(1)} async-done(((bf16[16,4,513]{2,1,0:T(4,128)(2,1)}), bf16[16,4,513]{2,1,0:T(4,128)(2,1)S(1)}, u32[]{:S(2)}, u32[]{:S(2)}) %all-to-all-start.1) | async-done | bytes 65696 | tf_op jit(solution)/shard_map/all_to_all | solution.py:14
  126.0 0.3 fusion.8
  126.6 14.3 %all_to_all.40 = bf16[16,4,128]{2,1,0:T(4,128)(2,1)S(1)} all-to-all(bf16[16,4,128]{2,1,0:T(4,128)(2,1)S(1)} %broadcast_in_dim.24), channel_id=1, replica_groups=mesh['grp'=2,'tp'=16,'y'=16,'c'=2] {'y'}, dimensions={0} | all-to-all | bytes 32768 | tf_op jit(solution)/shard_map/all_to_all | solution.py:14
  141.2 7.8 %all_to_all.41 = bf16[4,16,256]{2,1,0:T(8,128)(2,1)S(1)} all-to-all(bf16[4,16,256]{2,1,0:T(8,128)(2,1)S(1)} %pad_maximum_fusion.4), channel_id=1, replica_groups={{0,32,64,96},{128,160,192,224},{256,288,320,352},{384,416,448,480},{1,3..., dimensions={0} | all-to-all | bytes 65536 | tf_op jit(solution)/shard_map/all_to_all | solution.py:14
  149.0 16.0 %all_to_all.42 = bf16[16,16,256]{2,1,0:T(8,128)(2,1)S(1)} all-to-all(bf16[16,16,256]{2,1,0:T(8,128)(2,1)S(1)} %broadcast_in_dim.25), channel_id=1, replica_groups=mesh['grp'=2,'tp'=16,'y'=16,'c'=2] {'tp'}, dimensions={0} | all-to-all | bytes 262144 | tf_op jit(solution)/shard_map/all_to_all | solution.py:14
  165.1 0.2 convert_element_type.126
  165.3 0.1 fusion.14
  165.4 0.2 fusion.1
  165.6 0.7 pad_maximum_fusion.3
  166.3 3.9 %all-to-all-start.5 = ((bf16[16,4,513]{2,1,0:T(4,128)(2,1)}), bf16[16,4,513]{2,1,0:T(4,128)(2,1)S(1)}, u32[]{:S(2)}, u32[]{:S(2)}) async-start(bf16[16,4,513]{2,1,0:T(4,128)(2,1)} %pad_maximum_fusion.3), calls=%async_computation.5 | async-start | bytes 163840 | tf_op jit(solution)/shard_map/all_to_all | solution.py:14
  170.3 11.3 %all-to-all-done.5 = bf16[16,4,513]{2,1,0:T(4,128)(2,1)S(1)} async-done(((bf16[16,4,513]{2,1,0:T(4,128)(2,1)}), bf16[16,4,513]{2,1,0:T(4,128)(2,1)S(1)}, u32[]{:S(2)}, u32[]{:S(2)}) %all-to-all-start.5) | async-done | bytes 65696 | tf_op jit(solution)/shard_map/all_to_all | solution.py:14
  181.8 0.3 fusion.5
  182.3 0.6 broadcast_in_dim.26
  183.0 3.9 %all-to-all-start.6 = ((bf16[16,4,128]{2,1,0:T(4,128)(2,1)}), bf16[16,4,128]{2,1,0:T(4,128)(2,1)S(1)}, u32[]{:S(2)}, u32[]{:S(2)}) async-start(bf16[16,4,128]{2,1,0:T(4,128)(2,1)} %broadcast_in_dim.26), calls=%async_computation.6 | async-start | bytes 32768 | tf_op jit(solution)/shard_map/all_to_all | solution.py:14
  186.9 11.0 %all-to-all-done.6 = bf16[16,4,128]{2,1,0:T(4,128)(2,1)S(1)} async-done(((bf16[16,4,128]{2,1,0:T(4,128)(2,1)}), bf16[16,4,128]{2,1,0:T(4,128)(2,1)S(1)}, u32[]{:S(2)}, u32[]{:S(2)}) %all-to-all-start.6) | async-done | bytes 16416 | tf_op jit(solution)/shard_map/all_to_all | solution.py:14
  198.0 0.1 broadcast_select_fusion.3
  198.3 0.6 copy.112
  198.9 11.8 %all-to-all-start.7 = ((bf16[32,4,128]{2,1,0:T(4,128)(2,1)}), bf16[32,4,128]{2,1,0:T(4,128)(2,1)S(1)}, u32[]{:S(2)}, u32[]{:S(2)}) async-start(bf16[32,4,128]{2,1,0:T(4,128)(2,1)} %copy.112), calls=%async_computation.7 | async-start | bytes 65536 | tf_op jit(solution)/shard_map/all_to_all | solution.py:14
  210.8 0.3 multiply_add_fusion.1
  211.1 0.8 pad_maximum_fusion
  211.9 10.6 %all-to-all-done.7 = bf16[32,4,128]{2,1,0:T(4,128)(2,1)S(1)} async-done(((bf16[32,4,128]{2,1,0:T(4,128)(2,1)}), bf16[32,4,128]{2,1,0:T(4,128)(2,1)S(1)}, u32[]{:S(2)}, u32[]{:S(2)}) %all-to-all-start.7) | async-done | bytes 32800 | tf_op jit(solution)/shard_map/all_to_all | solution.py:14
  222.6 0.6 bitcast_reduce_fusion
  (48 shorter events, 2.0 us)
Async XLA Ops:
  0.6 88.7 %copy-start.2 = (bf16[2,128,128]{2,1,0:T(8,128)(2,1)S(1)}, bf16[2,128,128]{2,1,0:T(8,128)(2,1)}, u32[]{:S(2)}) copy-start(bf16[2,128,128]{2,1,0:T(8,128)(2,1)} %param.15) | copy-start | bytes 196612
  2.0 87.4 %copy-start.3 = (f32[2,128]{1,0:T(2,128)S(1)}, f32[2,128]{1,0:T(2,128)}, u32[]{:S(2)}) copy-start(f32[2,128]{1,0:T(2,128)} %param.11) | copy-start | bytes 3076
  2.0 99.5 %all-to-all-start = ((bf16[32,4,128]{2,1,0:T(4,128)(2,1)}), bf16[32,4,128]{2,1,0:T(4,128)(2,1)S(1)}, u32[]{:S(2)}, u32[]{:S(2)}) async-start(bf16[32,4,128]{2,1,0:T(4,128)(2,1)} %bitcast.3), calls=%async_computation | async-start | bytes 65536 | tf_op jit(solution)/shard_map/all_to_all | solution.py:14
  89.3 1.1 copy-start.1
  90.5 11.5 %collective-permute-start = (bf16[2,128,640]{2,1,0:T(8,128)(2,1)S(1)}, bf16[2,128,640]{2,1,0:T(8,128)(2,1)S(1)}, u32[]{:S(2)}, u32[]{:S(2)}) collective-permute-start(bf16[2,128,640]{2,1,0:T(8,128)(2,1)S(1)} %pad_maximum_fusion.1), channel_id=1, source_target_pairs={{0,1},{1,0},{2,3},{3,2},{4,5},{5,4},{6,7},{7,6},{8,9},{9,8},{10,11... | collective-permute-start | bytes 983048 | tf_op jit(solution)/shard_map/ppermute | solution.py:42
  101.9 24.1 %copy-start = (f32[2,4,1,128,128]{4,3,2,1,0:T(8,128)S(1)}, f32[2,4,1,128,128]{4,3,2,1,0:T(8,128)}, u32[]{:S(2)}) copy-start(f32[2,4,1,128,128]{4,3,2,1,0:T(8,128)} %param.19) | copy-start | bytes 1572868
  102.8 11.3 %copy-start.5 = (f32[2,128]{1,0:T(2,128)S(1)}, f32[2,128]{1,0:T(2,128)}, u32[]{:S(2)}) copy-start(f32[2,128]{1,0:T(2,128)} %param.17) | copy-start | bytes 3076
  102.8 23.0 %all-to-all-start.1 = ((bf16[16,4,513]{2,1,0:T(4,128)(2,1)}), bf16[16,4,513]{2,1,0:T(4,128)(2,1)S(1)}, u32[]{:S(2)}, u32[]{:S(2)}) async-start(bf16[16,4,513]{2,1,0:T(4,128)(2,1)} %pad_maximum_fusion.2), calls=%async_computation.1 | async-start | bytes 163840 | tf_op jit(solution)/shard_map/all_to_all | solution.py:14
  114.1 0.7 copy-start.4
  166.3 15.2 %all-to-all-start.5 = ((bf16[16,4,513]{2,1,0:T(4,128)(2,1)}), bf16[16,4,513]{2,1,0:T(4,128)(2,1)S(1)}, u32[]{:S(2)}, u32[]{:S(2)}) async-start(bf16[16,4,513]{2,1,0:T(4,128)(2,1)} %pad_maximum_fusion.3), calls=%async_computation.5 | async-start | bytes 163840 | tf_op jit(solution)/shard_map/all_to_all | solution.py:14
  183.0 14.9 %all-to-all-start.6 = ((bf16[16,4,128]{2,1,0:T(4,128)(2,1)}), bf16[16,4,128]{2,1,0:T(4,128)(2,1)S(1)}, u32[]{:S(2)}, u32[]{:S(2)}) async-start(bf16[16,4,128]{2,1,0:T(4,128)(2,1)} %broadcast_in_dim.26), calls=%async_computation.6 | async-start | bytes 32768 | tf_op jit(solution)/shard_map/all_to_all | solution.py:14
  198.9 23.6 %all-to-all-start.7 = ((bf16[32,4,128]{2,1,0:T(4,128)(2,1)}), bf16[32,4,128]{2,1,0:T(4,128)(2,1)S(1)}, u32[]{:S(2)}, u32[]{:S(2)}) async-start(bf16[32,4,128]{2,1,0:T(4,128)(2,1)} %copy.112), calls=%async_computation.7 | async-start | bytes 65536 | tf_op jit(solution)/shard_map/all_to_all | solution.py:14

commit v2 on v1

--- a/solution.py
+++ b/solution.py
@@ -42,6 +42,11 @@
     other = lax.ppermute(packed, "c", [(0, 1), (1, 0)])
     proj_width = joined.shape[2]
 
+    mine = (lax.broadcasted_iota(jnp.int32, (held, width), 0) // local_seqs == tp).astype(F32)
+    bounds = [jnp.broadcast_to(lower_bound[k], (local_seqs, lower_bound.shape[1])) for k in range(2)]
+    gains = [jnp.broadcast_to(head_gain[k], (local_seqs, head_count, HD)) for k in range(2)]
+    own, mate, mine, bounds, gains = lax.optimization_barrier((own, mate, mine, bounds, gains))
+
     updated = []
     for layer in range(2):
         own_f, mate_f = own.astype(F32), mate.astype(F32)
@@ -55,28 +60,34 @@
         query, forget_pre, value, gate_pre = (
             total[:, k * head_width : (k + 1) * head_width] * factor for k in range(4)
         )
-        bound = lower_bound[layer]
+        bound = bounds[layer]
         forget = bound + (1.0 - bound) * jax.nn.sigmoid(forget_pre)
         keyvec = (1.0 - bound) * jax.nn.sigmoid(-forget_pre)
 
         def shaped(array):
             return array.reshape(local_seqs, head_count, HD)
 
-        carried = (
-            shaped(forget)[..., None] * state[layer]
-            + shaped(keyvec)[..., None] * shaped(value)[..., None, :]
-        )
-        updated.append(carried)
+        def advance(forget, keyvec, value, layer=layer):
+            return (
+                shaped(forget)[..., None] * state[layer]
+                + shaped(keyvec)[..., None] * shaped(value)[..., None, :]
+            )
+
+        carried = advance(forget, keyvec, value)
+        updated.append((advance, (forget, keyvec, value)))
         readout = jnp.einsum("bhkv,bhk->bhv", carried, shaped(query))
         readout = (
             readout
             * lax.rsqrt(jnp.mean(readout * readout, axis=-1, keepdims=True) + 1e-06)
-            * head_gain[layer]
+            * gains[layer]
         )
         normed = (readout.reshape(local_seqs, head_count * HD) * jax.nn.sigmoid(gate_pre)).astype(
             BF16
         )
         got = exchange(jnp.broadcast_to(normed[None], (y_size, *normed.shape)), "y")
+        if layer == 1:
+            got, parts = lax.optimization_barrier((got, [p for _, p in updated]))
+            updated = [form(*p) for (form, _), p in zip(updated, parts)]
         gathered = got.reshape(held, head_count * HD)
         mixed_own = dot(gathered, packed[layer, :, proj_width:])
         mixed_mate = dot(gathered, other[layer, :, proj_width:])
@@ -92,9 +103,8 @@
             own = (own_f + mixed[:, :width]).astype(BF16)
             mate = (mate_f + mixed[:, width:]).astype(BF16)
         else:
-            mine = (jnp.arange(held) // local_seqs == tp)[:, None]
-            mixed_own = (mixed_own + jnp.where(mine, own_f, 0.0)).astype(BF16)
-            mixed_mate = (mixed_mate + jnp.where(mine, mate_f, 0.0)).astype(BF16)
+            mixed_own = (mixed_own + mine * own_f).astype(BF16)
+            mixed_mate = (mixed_mate + mine * mate_f).astype(BF16)
             first = jnp.where(core == 0, mixed_own, mixed_mate)
             second = jnp.where(core == 0, mixed_mate, mixed_own)
             sent = jnp.stack(

time: 224 us -> 221 us (0.987)
  blocking collectives: 38.1 us -> 90.2 us
  waiting for transfers between devices: 51.9 us -> 17.3 us
  starting transfers between devices: 121 us -> 102 us
    all_to_all x3 -> x6, blocking collectives: 38.1 us -> 90.2 us  [exchange(): return lax.all_to_all(x, axis, 0, 0, tiled=True, axis_index_groups=groups)]
    all_to_all x5 -> x2, waiting for transfers between devices: 51.9 us -> 17.3 us  [exchange(): return lax.all_to_all(x, axis, 0, 0, tiled=True, axis_index_groups=groups)]
    all_to_all x5 -> x2, starting transfers between devices: 118 us -> 98.8 us  [exchange(): return lax.all_to_all(x, axis, 0, 0, tiled=True, axis_index_groups=groups)]
  transfers between devices with their start and end apart: 6 -> 3, of which waited for: 5 -> 2; matrix products, arithmetic and copies ran while one was open for 1% -> 1% of each run, Pallas kernels for 0% -> 0%
where the time goes in v2:
time: 221 us; the launch traced here: 220 us
  starting transfers between devices  102 us (46%)
  blocking collectives  90.2 us (41%)
  waiting for transfers between devices  17.3 us (8%)
  other arithmetic  4.36 us (2%)
  local copies, waits for them, and re-layouts  3.73 us (2%)
    all_to_all x2, starting transfers between devices, exchange(): return lax.all_to_all(x, axis, 0, 0, tiled=True, axis_index_groups=groups)  98.8 us
    all_to_all x6, blocking collectives, exchange(): return lax.all_to_all(x, axis, 0, 0, tiled=True, axis_index_groups=groups)  90.2 us
    all_to_all x2, waiting for transfers between devices, exchange(): return lax.all_to_all(x, axis, 0, 0, tiled=True, axis_index_groups=groups)  17.3 us
  transfers between devices with their start and end apart: 3, of which 2 were waited for; matrix products, arithmetic and copies ran while one was open for 1% of the time, Pallas kernels for 0%

profile of v2, /device:TPU:5, one launch (start us, length us, event | category | flops | bytes accessed | tf_op | source)
XLA Modules:
  0.0 220.1 jit_solution(10743280731482312917)
XLA Ops:
  0.6 1.3 broadcast_in_dim.19
  2.0 87.3 %all-to-all-start = ((bf16[32,4,128]{2,1,0:T(4,128)(2,1)}), bf16[32,4,128]{2,1,0:T(4,128)(2,1)S(1)}, u32[]{:S(2)}, u32[]{:S(2)}) async-start(bf16[32,4,128]{2,1,0:T(4,128)(2,1)} %bitcast.1), calls=%async_computation | async-start | bytes 65536 | tf_op jit(solution)/shard_map/all_to_all | solution.py:14
  89.4 1.0 multiply_convert_fusion
  90.5 3.0 %collective-permute-start = (bf16[2,128,640]{2,1,0:T(8,128)(2,1)S(1)}, bf16[2,128,640]{2,1,0:T(8,128)(2,1)S(1)}, u32[]{:S(2)}, u32[]{:S(2)}) collective-permute-start(bf16[2,128,640]{2,1,0:T(8,128)(2,1)S(1)} %pad_maximum_fusion.1), channel_id=1, source_target_pairs={{0,1},{1,0},{2,3},{3,2},{4,5},{5,4},{6,7},{7,6},{8,9},{9,8},{10,11... | collective-permute-start | bytes 983048 | tf_op jit(solution)/shard_map/ppermute | solution.py:42
  93.5 0.7 copy-done.4
  94.3 0.6 copy-done.5
  94.8 6.6 %all-to-all-done = bf16[32,4,128]{2,1,0:T(4,128)(2,1)S(1)} async-done(((bf16[32,4,128]{2,1,0:T(4,128)(2,1)}), bf16[32,4,128]{2,1,0:T(4,128)(2,1)S(1)}, u32[]{:S(2)}, u32[]{:S(2)}) %all-to-all-start) | async-done | bytes 32800 | tf_op jit(solution)/shard_map/all_to_all | solution.py:14
  101.8 0.2 convert_element_type.117
  101.9 0.1 fusion.15
  102.1 0.1 fusion
  102.3 22.6 %all_to_all.40 = bf16[16,4,513]{2,1,0:T(4,128)(2,1)S(1)} all-to-all(bf16[16,4,513]{2,1,0:T(4,128)(2,1)S(1)} %pad_maximum_fusion.2), channel_id=1, replica_groups=mesh['grp'=2,'tp'=16,'y'=16,'c'=2] {'y'}, dimensions={0} | all-to-all | bytes 131328 | tf_op jit(solution)/shard_map/all_to_all | solution.py:14
  125.0 0.1 fusion.46
  125.2 0.3 fusion.8
  125.8 14.3 %all_to_all.41 = bf16[16,4,128]{2,1,0:T(4,128)(2,1)S(1)} all-to-all(bf16[16,4,128]{2,1,0:T(4,128)(2,1)S(1)} %broadcast_in_dim.48), channel_id=1, replica_groups=mesh['grp'=2,'tp'=16,'y'=16,'c'=2] {'y'}, dimensions={0} | all-to-all | bytes 32768 | tf_op jit(solution)/shard_map/all_to_all | solution.py:14
  140.1 0.1 convolution_convert_fusion.1
  140.2 0.1 convolution_convert_fusion
  140.4 7.8 %all_to_all.42 = bf16[4,16,256]{2,1,0:T(8,128)(2,1)S(1)} all-to-all(bf16[4,16,256]{2,1,0:T(8,128)(2,1)S(1)} %pad_maximum_fusion.4), channel_id=1, replica_groups={{0,32,64,96},{128,160,192,224},{256,288,320,352},{384,416,448,480},{1,3..., dimensions={0} | all-to-all | bytes 65536 | tf_op jit(solution)/shard_map/all_to_all | solution.py:14
  148.2 16.7 %all_to_all.43 = bf16[16,16,256]{2,1,0:T(8,128)(2,1)S(1)} all-to-all(bf16[16,16,256]{2,1,0:T(8,128)(2,1)S(1)} %broadcast_in_dim.49), channel_id=1, replica_groups=mesh['grp'=2,'tp'=16,'y'=16,'c'=2] {'tp'}, dimensions={0} | all-to-all | bytes 262144 | tf_op jit(solution)/shard_map/all_to_all | solution.py:14
  165.0 0.1 fusion.14
  165.1 0.1 fusion.1
  165.3 0.1 convert_element_type.118
  165.5 14.4 %all_to_all.44 = bf16[16,4,513]{2,1,0:T(4,128)(2,1)S(1)} all-to-all(bf16[16,4,513]{2,1,0:T(4,128)(2,1)S(1)} %pad_maximum_fusion.3), channel_id=1, replica_groups=mesh['grp'=2,'tp'=16,'y'=16,'c'=2] {'y'}, dimensions={0} | all-to-all | bytes 131328 | tf_op jit(solution)/shard_map/all_to_all | solution.py:14
  180.1 0.3 fusion.5
  180.7 14.5 %all_to_all.45 = bf16[16,4,128]{2,1,0:T(4,128)(2,1)S(1)} all-to-all(bf16[16,4,128]{2,1,0:T(4,128)(2,1)S(1)} %broadcast_in_dim.50), channel_id=1, replica_groups=mesh['grp'=2,'tp'=16,'y'=16,'c'=2] {'y'}, dimensions={0} | all-to-all | bytes 32768 | tf_op jit(solution)/shard_map/all_to_all | solution.py:14
  195.2 0.1 fusion.2
  195.3 0.1 broadcast_select_fusion.3
  195.6 0.6 copy.94
  196.2 11.5 %all-to-all-start.7 = ((bf16[32,4,128]{2,1,0:T(4,128)(2,1)}), bf16[32,4,128]{2,1,0:T(4,128)(2,1)S(1)}, u32[]{:S(2)}, u32[]{:S(2)}) async-start(bf16[32,4,128]{2,1,0:T(4,128)(2,1)} %copy.94), calls=%async_computation.7 | async-start | bytes 65536 | tf_op jit(solution)/shard_map/all_to_all | solution.py:14
  207.7 0.3 multiply_add_fusion.1
  208.0 0.8 pad_maximum_fusion
  208.9 10.6 %all-to-all-done.7 = bf16[32,4,128]{2,1,0:T(4,128)(2,1)S(1)} async-done(((bf16[32,4,128]{2,1,0:T(4,128)(2,1)}), bf16[32,4,128]{2,1,0:T(4,128)(2,1)S(1)}, u32[]{:S(2)}, u32[]{:S(2)}) %all-to-all-start.7) | async-done | bytes 32800 | tf_op jit(solution)/shard_map/all_to_all | solution.py:14
  219.5 0.6 bitcast_reduce_fusion
  (51 shorter events, 1.7 us)
Async XLA Ops:
  0.6 88.7 %copy-start.2 = (bf16[2,128,128]{2,1,0:T(8,128)(2,1)S(1)}, bf16[2,128,128]{2,1,0:T(8,128)(2,1)}, u32[]{:S(2)}) copy-start(bf16[2,128,128]{2,1,0:T(8,128)(2,1)} %param.15) | copy-start | bytes 196612
  2.0 87.4 %copy-start.3 = (f32[2,128]{1,0:T(2,128)S(1)}, f32[2,128]{1,0:T(2,128)}, u32[]{:S(2)}) copy-start(f32[2,128]{1,0:T(2,128)} %param.11) | copy-start | bytes 3076
  2.0 99.5 %all-to-all-start = ((bf16[32,4,128]{2,1,0:T(4,128)(2,1)}), bf16[32,4,128]{2,1,0:T(4,128)(2,1)S(1)}, u32[]{:S(2)}, u32[]{:S(2)}) async-start(bf16[32,4,128]{2,1,0:T(4,128)(2,1)} %bitcast.1), calls=%async_computation | async-start | bytes 65536 | tf_op jit(solution)/shard_map/all_to_all | solution.py:14
  89.3 1.1 copy-start.1
  90.5 11.6 %collective-permute-start = (bf16[2,128,640]{2,1,0:T(8,128)(2,1)S(1)}, bf16[2,128,640]{2,1,0:T(8,128)(2,1)S(1)}, u32[]{:S(2)}, u32[]{:S(2)}) collective-permute-start(bf16[2,128,640]{2,1,0:T(8,128)(2,1)S(1)} %pad_maximum_fusion.1), channel_id=1, source_target_pairs={{0,1},{1,0},{2,3},{3,2},{4,5},{5,4},{6,7},{7,6},{8,9},{9,8},{10,11... | collective-permute-start | bytes 983048 | tf_op jit(solution)/shard_map/ppermute | solution.py:42
  93.5 0.7 copy-start.4
  94.2 0.7 copy-start.5
  102.1 23.1 %copy-start = (f32[2,4,1,128,128]{4,3,2,1,0:T(8,128)S(1)}, f32[2,4,1,128,128]{4,3,2,1,0:T(8,128)}, u32[]{:S(2)}) copy-start(f32[2,4,1,128,128]{4,3,2,1,0:T(8,128)} %param.19) | copy-start | bytes 1572868
  196.2 23.3 %all-to-all-start.7 = ((bf16[32,4,128]{2,1,0:T(4,128)(2,1)}), bf16[32,4,128]{2,1,0:T(4,128)(2,1)S(1)}, u32[]{:S(2)}, u32[]{:S(2)}) async-start(bf16[32,4,128]{2,1,0:T(4,128)(2,1)} %copy.94), calls=%async_computation.7 | async-start | bytes 65536 | tf_op jit(solution)/shard_map/all_to_all | solution.py:14

commit v3 on v2

v3 whole, which is shorter than its diff:
```python
import jax
import jax.numpy as jnp
from jax import lax
from jax.sharding import Mesh, PartitionSpec as P

D = 4096
HD = 128
NEAR = 2
TP = ("far", "near")
BF16 = jnp.bfloat16
F32 = jnp.float32


def exchange(x, axis):
    return lax.all_to_all(x, axis, 0, 0, tiled=True)


def dot(a, b):
    return jnp.dot(a, b, preferred_element_type=F32)


def per_device(
    tokens, norm_gain, w_query, w_forget, w_value, w_gate, lower_bound, head_gain, w_out, state
):
    rows, width = tokens.shape
    local_seqs, head_count = state.shape[1:3]
    tp_size, y_size, c_size = (lax.axis_size(a) for a in (TP, "y", "c"))
    assert c_size == 2 and rows == c_size * local_seqs and tp_size == y_size
    tp, core, side = (lax.axis_index(a) for a in (TP, "c", "near"))
    held = y_size * local_seqs

    sent = jnp.broadcast_to(
        tokens.reshape(1, c_size, local_seqs, width), (tp_size, c_size, local_seqs, width)
    )
    got = exchange(sent.reshape(tp_size * c_size, local_seqs, width), (*TP, "c"))
    got = got.reshape(tp_size, c_size, local_seqs, width)
    own = jnp.where(core == 0, got[:, 0], got[:, 1]).reshape(held, width)
    mate = jnp.where(core == 0, got[:, 1], got[:, 0]).reshape(held, width)

    joined = jnp.concatenate([w_query, w_forget, w_value, w_gate], axis=2)
    joined = (joined.astype(F32) * norm_gain[:, :, None]).astype(BF16)
    packed = jnp.concatenate([joined, w_out], axis=2)
    other = lax.ppermute(packed, "c", [(0, 1), (1, 0)])
    proj_width = joined.shape[2]

    pair_out = jnp.concatenate([w_out[0], other[0, :, proj_width:]], axis=1)
    near_out = lax.ppermute(pair_out, "near", [(0, 1), (1, 0)])

    mine = (lax.broadcasted_iota(jnp.int32, (held, width), 0) // local_seqs == tp).astype(F32)
    bounds = [jnp.broadcast_to(lower_bound[k], (local_seqs, lower_bound.shape[1])) for k in range(2)]
    gains = [jnp.broadcast_to(head_gain[k], (local_seqs, head_count, HD)) for k in range(2)]
    own, mate, mine, bounds, gains, pair_out, near_out, side = lax.optimization_barrier(
        (own, mate, mine, bounds, gains, pair_out, near_out, side)
    )

    updated = []
    for layer in range(2):
        own_f, mate_f = own.astype(F32), mate.astype(F32)
        squares = jnp.sum(own_f * own_f + mate_f * mate_f, axis=1, keepdims=True)
        partial = dot(own, packed[layer, :, :proj_width]) + dot(mate, other[layer, :, :proj_width])
        payload = jnp.concatenate([partial.astype(BF16), squares.astype(BF16)], axis=1)
        got = exchange(payload.reshape(y_size, local_seqs, proj_width + 1), "y")
        total = jnp.sum(got.astype(F32), axis=0)
        factor = lax.rsqrt(total[:, proj_width:] / D + 1e-06)
        head_width = proj_width // 4
        query, forget_pre, value, gate_pre = (
            total[:, k * head_width : (k + 1) * head_width] * factor for k in range(4)
        )
        bound = bounds[layer]
        forget = bound + (1.0 - bound) * jax.nn.sigmoid(forget_pre)
        keyvec = (1.0 - bound) * jax.nn.sigmoid(-forget_pre)

        def shaped(array):
            return array.reshape(local_seqs, head_count, HD)

        def advance(forget, keyvec, value, layer=layer):
            return (
                shaped(forget)[..., None] * state[layer]
                + shaped(keyvec)[..., None] * shaped(value)[..., None, :]
            )

        carried = advance(forget, keyvec, value)
        updated.append((advance, (forget, keyvec, value)))
        readout = jnp.einsum("bhkv,bhk->bhv", carried, shaped(query))
        readout = (
            readout
            * lax.rsqrt(jnp.mean(readout * readout, axis=-1, keepdims=True) + 1e-06)
            * gains[layer]
        )
        normed = (readout.reshape(local_seqs, head_count * HD) * jax.nn.sigmoid(gate_pre)).astype(
            BF16
        )
        if layer == 0:
            got = exchange(
                jnp.broadcast_to(normed[None], (NEAR * y_size, *normed.shape)), ("near", "y")
            ).reshape(NEAR, NEAR, held // NEAR, head_count * HD)
            part = jnp.where(side == 0, got[:, 0], got[:, 1])
            mixed = dot(jnp.where(side == 0, part[0], part[1]), pair_out)
            mixed = mixed + dot(jnp.where(side == 0, part[1], part[0]), near_out)
            piece = mixed.astype(BF16)
            got = exchange(jnp.broadcast_to(piece[None], (tp_size, *piece.shape)), TP)
            got = got.reshape(tp_size // NEAR, NEAR, held // NEAR, 2 * width)
            mixed = jnp.sum(got.astype(F32), axis=0).reshape(held, 2 * width)
            own = (own_f + mixed[:, :width]).astype(BF16)
            mate = (mate_f + mixed[:, width:]).astype(BF16)
        else:
            got = exchange(jnp.broadcast_to(normed[None], (y_size, *normed.shape)), "y")
            got, parts = lax.optimization_barrier((got, [p for _, p in updated]))
            updated = [form(*p) for (form, _), p in zip(updated, parts)]
            gathered = got.reshape(held, head_count * HD)
            mixed_own = dot(gathered, packed[layer, :, proj_width:])
            mixed_mate = dot(gathered, other[layer, :, proj_width:])
            mixed_own = (mixed_own + mine * own_f).astype(BF16)
            mixed_mate = (mixed_mate + mine * mate_f).astype(BF16)
            first = jnp.where(core == 0, mixed_own, mixed_mate)
            second = jnp.where(core == 0, mixed_mate, mixed_own)
            sent = jnp.stack(
                [a.reshape(tp_size, local_seqs, width) for a in (first, second)], axis=1
            )
            got = exchange(sent.reshape(tp_size * c_size, local_seqs, width), (*TP, "c"))
            got = got.reshape(tp_size, rows, width)
            hidden = jnp.sum(got.astype(F32), axis=0).astype(BF16)
    return (hidden, jnp.stack(updated))


def solution(mesh):
    grp, tp, dp = mesh.devices.shape
    fine = Mesh(
        mesh.devices.reshape(grp, tp // NEAR, NEAR, dp // 2, 2), ("grp", "far", "near", "y", "c")
    )
    tps, dps = ("far", "near"), ("y", "c")
    weight = P(None, dps, tps)
    held = P(None, ("grp", *dps), tps, None, None)
    return jax.shard_map(
        per_device,
        mesh=fine,
        in_specs=(
            P(("grp", *tps), dps),
            P(None, dps),
            weight,
            weight,
            weight,
            weight,
            P(None, tps),
            P(),
            P(None, tps, dps),
            held,
        ),
        out_specs=(P(("grp", *tps), dps), held),
        check_vma=False,
    )
```

time: 221 us -> 225 us (1.018)
  blocking collectives: 90.2 us -> 68.6 us
  waiting for transfers between devices: 17.3 us -> 31.8 us
  starting transfers between devices: 102 us -> 113 us
    all_to_all x6 -> x4, blocking collectives: 90.2 us -> 68.6 us  [exchange(): return lax.all_to_all(x, axis, 0, 0, tiled=True)]
    all_to_all x2 -> x3, waiting for transfers between devices: 17.3 us -> 29.1 us  [exchange(): return lax.all_to_all(x, axis, 0, 0, tiled=True)]
    all_to_all x2 -> x3, starting transfers between devices: 98.8 us -> 107 us  [exchange(): return lax.all_to_all(x, axis, 0, 0, tiled=True)]
    ppermute x0 -> x1, waiting for transfers between devices: none -> 2.69 us  [per_device(): near_out = lax.ppermute(pair_out, 'near', [(0, 1), (1, 0)])]
  transfers between devices with their start and end apart: 3 -> 5, of which waited for: 2 -> 4; matrix products, arithmetic and copies ran while one was open for 1% -> 1% of each run, Pallas kernels for 0% -> 0%
where the time goes in v3:
time: 225 us; the launch traced here: 224 us
  starting transfers between devices  113 us (50%)
  blocking collectives  68.6 us (30%)
  waiting for transfers between devices  31.8 us (14%)
  local copies, waits for them, and re-layouts  4.39 us (2%)
  other arithmetic  4.38 us (2%)
    all_to_all x3, starting transfers between devices, exchange(): return lax.all_to_all(x, axis, 0, 0, tiled=True)  107 us
    all_to_all x4, blocking collectives, exchange(): return lax.all_to_all(x, axis, 0, 0, tiled=True)  68.6 us
    all_to_all x3, waiting for transfers between devices, exchange(): return lax.all_to_all(x, axis, 0, 0, tiled=True)  29.1 us
  transfers between devices with their start and end apart: 5, of which 4 were waited for; matrix products, arithmetic and copies ran while one was open for 1% of the time, Pallas kernels for 0%

profile of v3, /device:TPU:5, one launch (start us, length us, event | category | flops | bytes accessed | tf_op | source)
XLA Modules:
  0.0 224.4 jit_solution(8549753253867825283)
XLA Ops:
  0.6 1.3 broadcast_in_dim.19
  2.0 87.3 %all-to-all-start = ((bf16[32,4,128]{2,1,0:T(4,128)(2,1)}), bf16[32,4,128]{2,1,0:T(4,128)(2,1)S(1)}, u32[]{:S(2)}, u32[]{:S(2)}) async-start(bf16[32,4,128]{2,1,0:T(4,128)(2,1)} %bitcast.1), calls=%async_computation | async-start | bytes 65536 | tf_op jit(solution)/shard_map/all_to_all | solution.py:15
  89.4 1.0 multiply_convert_fusion
  90.5 3.0 %collective-permute-start = (bf16[2,128,640]{2,1,0:T(8,128)(2,1)S(1)}, bf16[2,128,640]{2,1,0:T(8,128)(2,1)S(1)}, u32[]{:S(2)}, u32[]{:S(2)}) collective-permute-start(bf16[2,128,640]{2,1,0:T(8,128)(2,1)S(1)} %pad_maximum_fusion.1), channel_id=1, source_target_pairs={{0,1},{1,0},{2,3},{3,2},{4,5},{5,4},{6,7},{7,6},{8,9},{9,8},{10,11... | collective-permute-start | bytes 983048 | tf_op jit(solution)/shard_map/ppermute | solution.py:43
  93.6 0.6 copy-done.4
  94.2 0.7 copy-done.5
  94.9 6.6 %all-to-all-done = bf16[32,4,128]{2,1,0:T(4,128)(2,1)S(1)} async-done(((bf16[32,4,128]{2,1,0:T(4,128)(2,1)}), bf16[32,4,128]{2,1,0:T(4,128)(2,1)S(1)}, u32[]{:S(2)}, u32[]{:S(2)}) %all-to-all-start) | async-done | bytes 32800 | tf_op jit(solution)/shard_map/all_to_all | solution.py:15
  101.5 2.2 collective-permute-start.1
  103.9 2.7 %collective-permute-done.1 = bf16[128,256]{1,0:T(8,128)(2,1)S(1)} collective-permute-done((bf16[128,256]{1,0:T(8,128)(2,1)S(1)}, bf16[128,256]{1,0:T(8,128)(2,1)S(1)}, u32[]{:S(2)}, u32[]{:S(2)}) %collective-permute-start.1) | collective-permute-done | bytes 65568 | tf_op jit(solution)/shard_map/ppermute | solution.py:47
  106.7 0.2 convert_element_type.117
  106.8 0.1 fusion.15
  107.0 0.1 fusion
  107.2 22.5 %all_to_all.35 = bf16[16,4,513]{2,1,0:T(4,128)(2,1)S(1)} all-to-all(bf16[16,4,513]{2,1,0:T(4,128)(2,1)S(1)} %pad_maximum_fusion.2), channel_id=1, replica_groups=mesh['grp'=2,'far'=8,'near'=2,'y'=16,'c'=2] {'y'}, dimensions={0} | all-to-all | bytes 131328 | tf_op jit(solution)/shard_map/all_to_all | solution.py:15
  130.0 0.3 fusion.8
  130.6 0.6 broadcast_in_dim.48
  131.2 4.8 %all-to-all-start.2 = ((bf16[32,4,128]{2,1,0:T(4,128)(2,1)}), bf16[32,4,128]{2,1,0:T(4,128)(2,1)S(1)}, u32[]{:S(2)}, u32[]{:S(2)}) async-start(bf16[32,4,128]{2,1,0:T(4,128)(2,1)} %broadcast_in_dim.48), calls=%async_computation.2 | async-start | bytes 65536 | tf_op jit(solution)/shard_map/all_to_all | solution.py:15
  136.0 11.9 %all-to-all-done.2 = bf16[32,4,128]{2,1,0:T(4,128)(2,1)S(1)} async-done(((bf16[32,4,128]{2,1,0:T(4,128)(2,1)}), bf16[32,4,128]{2,1,0:T(4,128)(2,1)S(1)}, u32[]{:S(2)}, u32[]{:S(2)}) %all-to-all-start.2) | async-done | bytes 32800 | tf_op jit(solution)/shard_map/all_to_all | solution.py:15
  148.0 0.1 fusion.2
  148.2 17.5 %all_to_all.36 = bf16[16,32,256]{2,1,0:T(8,128)(2,1)S(1)} all-to-all(bf16[16,32,256]{2,1,0:T(8,128)(2,1)S(1)} %broadcast_in_dim.49), channel_id=1, replica_groups=mesh['grp'=2,'far'=8,'near'=2,'y'=16,'c'=2] {'far','near'}, dimensions={0} | all-to-all | bytes 524288 | tf_op jit(solution)/shard_map/all_to_all | solution.py:15
  165.8 0.1 fusion.14
  166.0 0.2 fusion.1
  166.2 0.1 convert_element_type.118
  166.4 14.4 %all_to_all.37 = bf16[16,4,513]{2,1,0:T(4,128)(2,1)S(1)} all-to-all(bf16[16,4,513]{2,1,0:T(4,128)(2,1)S(1)} %pad_maximum_fusion.3), channel_id=1, replica_groups=mesh['grp'=2,'far'=8,'near'=2,'y'=16,'c'=2] {'y'}, dimensions={0} | all-to-all | bytes 131328 | tf_op jit(solution)/shard_map/all_to_all | solution.py:15
  181.0 0.3 fusion.5
  181.5 14.2 %all_to_all.38 = bf16[16,4,128]{2,1,0:T(4,128)(2,1)S(1)} all-to-all(bf16[16,4,128]{2,1,0:T(4,128)(2,1)S(1)} %broadcast_in_dim.50), channel_id=1, replica_groups=mesh['grp'=2,'far'=8,'near'=2,'y'=16,'c'=2] {'y'}, dimensions={0} | all-to-all | bytes 32768 | tf_op jit(solution)/shard_map/all_to_all | solution.py:15
  195.9 0.1 broadcast_select_fusion.3
  196.2 0.6 copy.94
  196.8 15.2 %all-to-all-start.6 = ((bf16[32,4,128]{2,1,0:T(4,128)(2,1)}), bf16[32,4,128]{2,1,0:T(4,128)(2,1)S(1)}, u32[]{:S(2)}, u32[]{:S(2)}) async-start(bf16[32,4,128]{2,1,0:T(4,128)(2,1)} %copy.94), calls=%async_computation.6 | async-start | bytes 65536 | tf_op jit(solution)/shard_map/all_to_all | solution.py:15
  212.0 0.3 multiply_add_fusion.1
  212.4 0.8 pad_maximum_fusion
  213.2 10.6 %all-to-all-done.6 = bf16[32,4,128]{2,1,0:T(4,128)(2,1)S(1)} async-done(((bf16[32,4,128]{2,1,0:T(4,128)(2,1)}), bf16[32,4,128]{2,1,0:T(4,128)(2,1)S(1)}, u32[]{:S(2)}, u32[]{:S(2)}) %all-to-all-start.6) | async-done | bytes 32800 | tf_op jit(solution)/shard_map/all_to_all | solution.py:15
  223.8 0.6 bitcast_reduce_fusion
  (55 shorter events, 2.1 us)
Async XLA Ops:
  0.6 88.7 %copy-start.2 = (bf16[2,128,128]{2,1,0:T(8,128)(2,1)S(1)}, bf16[2,128,128]{2,1,0:T(8,128)(2,1)}, u32[]{:S(2)}) copy-start(bf16[2,128,128]{2,1,0:T(8,128)(2,1)} %param.15) | copy-start | bytes 196612
  2.0 87.4 %copy-start.3 = (f32[2,128]{1,0:T(2,128)S(1)}, f32[2,128]{1,0:T(2,128)}, u32[]{:S(2)}) copy-start(f32[2,128]{1,0:T(2,128)} %param.11) | copy-start | bytes 3076
  2.0 99.5 %all-to-all-start = ((bf16[32,4,128]{2,1,0:T(4,128)(2,1)}), bf16[32,4,128]{2,1,0:T(4,128)(2,1)S(1)}, u32[]{:S(2)}, u32[]{:S(2)}) async-start(bf16[32,4,128]{2,1,0:T(4,128)(2,1)} %bitcast.1), calls=%async_computation | async-start | bytes 65536 | tf_op jit(solution)/shard_map/all_to_all | solution.py:15
  89.3 1.1 copy-start.1
  90.5 11.0 %collective-permute-start = (bf16[2,128,640]{2,1,0:T(8,128)(2,1)S(1)}, bf16[2,128,640]{2,1,0:T(8,128)(2,1)S(1)}, u32[]{:S(2)}, u32[]{:S(2)}) collective-permute-start(bf16[2,128,640]{2,1,0:T(8,128)(2,1)S(1)} %pad_maximum_fusion.1), channel_id=1, source_target_pairs={{0,1},{1,0},{2,3},{3,2},{4,5},{5,4},{6,7},{7,6},{8,9},{9,8},{10,11... | collective-permute-start | bytes 983048 | tf_op jit(solution)/shard_map/ppermute | solution.py:43
  93.5 0.7 copy-start.4
  94.2 0.7 copy-start.5
  101.5 5.0 %collective-permute-start.1 = (bf16[128,256]{1,0:T(8,128)(2,1)S(1)}, bf16[128,256]{1,0:T(8,128)(2,1)S(1)}, u32[]{:S(2)}, u32[]{:S(2)}) collective-permute-start(bf16[128,256]{1,0:T(8,128)(2,1)S(1)} %pad_maximum_fusion.4), channel_id=1, source_target_pairs={{0,32},{32,0},{1,33},{33,1},{2,34},{34,2},{3,35},{35,3},{4,36},{36... | collective-permute-start | bytes 196616 | tf_op jit(solution)/shard_map/ppermute | solution.py:47
  107.0 23.0 %copy-start = (f32[2,4,1,128,128]{4,3,2,1,0:T(8,128)S(1)}, f32[2,4,1,128,128]{4,3,2,1,0:T(8,128)}, u32[]{:S(2)}) copy-start(f32[2,4,1,128,128]{4,3,2,1,0:T(8,128)} %param.19) | copy-start | bytes 1572868
  131.2 16.6 %all-to-all-start.2 = ((bf16[32,4,128]{2,1,0:T(4,128)(2,1)}), bf16[32,4,128]{2,1,0:T(4,128)(2,1)S(1)}, u32[]{:S(2)}, u32[]{:S(2)}) async-start(bf16[32,4,128]{2,1,0:T(4,128)(2,1)} %broadcast_in_dim.48), calls=%async_computation.2 | async-start | bytes 65536 | tf_op jit(solution)/shard_map/all_to_all | solution.py:15
  196.8 27.0 %all-to-all-start.6 = ((bf16[32,4,128]{2,1,0:T(4,128)(2,1)}), bf16[32,4,128]{2,1,0:T(4,128)(2,1)S(1)}, u32[]{:S(2)}, u32[]{:S(2)}) async-start(bf16[32,4,128]{2,1,0:T(4,128)(2,1)} %copy.94), calls=%async_computation.6 | async-start | bytes 65536 | tf_op jit(solution)/shard_map/all_to_all | solution.py:15

commit v4 on v2

--- a/solution.py
+++ b/solution.py
@@ -47,7 +47,7 @@
     gains = [jnp.broadcast_to(head_gain[k], (local_seqs, head_count, HD)) for k in range(2)]
     own, mate, mine, bounds, gains = lax.optimization_barrier((own, mate, mine, bounds, gains))
 
-    updated = []
+    steps = []
     for layer in range(2):
         own_f, mate_f = own.astype(F32), mate.astype(F32)
         squares = jnp.sum(own_f * own_f + mate_f * mate_f, axis=1, keepdims=True)
@@ -67,14 +67,12 @@
         def shaped(array):
             return array.reshape(local_seqs, head_count, HD)
 
-        def advance(forget, keyvec, value, layer=layer):
-            return (
-                shaped(forget)[..., None] * state[layer]
-                + shaped(keyvec)[..., None] * shaped(value)[..., None, :]
-            )
+        def advance(forget, keyvec, value, old):
+            return forget[..., None] * old + keyvec[..., None] * value[..., None, :]
 
-        carried = advance(forget, keyvec, value)
-        updated.append((advance, (forget, keyvec, value)))
+        step = [shaped(a) for a in (forget, keyvec, value)]
+        steps.append(step)
+        carried = advance(*step, state[layer])
         readout = jnp.einsum("bhkv,bhk->bhv", carried, shaped(query))
         readout = (
             readout
@@ -85,9 +83,6 @@
             BF16
         )
         got = exchange(jnp.broadcast_to(normed[None], (y_size, *normed.shape)), "y")
-        if layer == 1:
-            got, parts = lax.optimization_barrier((got, [p for _, p in updated]))
-            updated = [form(*p) for (form, _), p in zip(updated, parts)]
         gathered = got.reshape(held, head_count * HD)
         mixed_own = dot(gathered, packed[layer, :, proj_width:])
         mixed_mate = dot(gathered, other[layer, :, proj_width:])
@@ -111,9 +106,11 @@
                 [a.reshape(tp_size, local_seqs, width) for a in (first, second)], axis=1
             )
             got = exchange(sent.reshape(tp_size * c_size, local_seqs, width), ("tp", "c"))
+            got, steps = lax.optimization_barrier((got, steps))
             got = got.reshape(tp_size, rows, width)
             hidden = jnp.sum(got.astype(F32), axis=0).astype(BF16)
-    return (hidden, jnp.stack(updated))
+    moved = advance(*(jnp.stack(pair) for pair in zip(*steps)), state)
+    return (hidden, moved)
 
 
 def solution(mesh):

time: 221 us -> 221 us (level)
  blocking collectives: 90.2 us -> 113 us
  starting transfers between devices: 102 us -> 90.3 us
  waiting for transfers between devices: 17.3 us -> 6.64 us
    all_to_all x6 -> x7, blocking collectives: 90.2 us -> 113 us  [exchange(): return lax.all_to_all(x, axis, 0, 0, tiled=True, axis_index_groups=groups)]
    all_to_all x2 -> x1, starting transfers between devices: 98.8 us -> 87.3 us  [exchange(): return lax.all_to_all(x, axis, 0, 0, tiled=True, axis_index_groups=groups)]
    all_to_all x2 -> x1, waiting for transfers between devices: 17.3 us -> 6.64 us  [exchange(): return lax.all_to_all(x, axis, 0, 0, tiled=True, axis_index_groups=groups)]
  transfers between devices with their start and end apart: 3 -> 2, of which waited for: 2 -> 1; matrix products, arithmetic and copies ran while one was open for 1% -> 1% of each run, Pallas kernels for 0% -> 0%
where the time goes in v4:
time: 221 us; the launch traced here: 220 us
  blocking collectives  113 us (51%)
  starting transfers between devices  90.3 us (41%)
  waiting for transfers between devices  6.64 us (3%)
  other arithmetic  4.34 us (2%)
  local copies, waits for them, and re-layouts  3.13 us (1%)
    all_to_all x7, blocking collectives, exchange(): return lax.all_to_all(x, axis, 0, 0, tiled=True, axis_index_groups=groups)  113 us
    all_to_all x1, starting transfers between devices, exchange(): return lax.all_to_all(x, axis, 0, 0, tiled=True, axis_index_groups=groups)  87.3 us
    all_to_all x1, waiting for transfers between devices, exchange(): return lax.all_to_all(x, axis, 0, 0, tiled=True, axis_index_groups=groups)  6.64 us
  transfers between devices with their start and end apart: 2, of which 1 were waited for; matrix products, arithmetic and copies ran while one was open for 1% of the time, Pallas kernels for 0%

profile of v4, /device:TPU:5, one launch (start us, length us, event | category | flops | bytes accessed | tf_op | source)
XLA Modules:
  0.0 220.4 jit_solution(8095025494342053280)
XLA Ops:
  0.6 1.3 broadcast_in_dim.19
  2.0 87.3 %all-to-all-start = ((bf16[32,4,128]{2,1,0:T(4,128)(2,1)}), bf16[32,4,128]{2,1,0:T(4,128)(2,1)S(1)}, u32[]{:S(2)}, u32[]{:S(2)}) async-start(bf16[32,4,128]{2,1,0:T(4,128)(2,1)} %bitcast.1), calls=%async_computation | async-start | bytes 65536 | tf_op jit(solution)/shard_map/all_to_all | solution.py:14
  89.4 1.0 multiply_convert_fusion
  90.5 3.0 %collective-permute-start = (bf16[2,128,640]{2,1,0:T(8,128)(2,1)S(1)}, bf16[2,128,640]{2,1,0:T(8,128)(2,1)S(1)}, u32[]{:S(2)}, u32[]{:S(2)}) collective-permute-start(bf16[2,128,640]{2,1,0:T(8,128)(2,1)S(1)} %pad_maximum_fusion), channel_id=1, source_target_pairs={{0,1},{1,0},{2,3},{3,2},{4,5},{5,4},{6,7},{7,6},{8,9},{9,8},{10,11... | collective-permute-start | bytes 983048 | tf_op jit(solution)/shard_map/ppermute | solution.py:42
  93.5 0.7 copy-done.4
  94.3 0.6 copy-done.5
  94.8 6.6 %all-to-all-done = bf16[32,4,128]{2,1,0:T(4,128)(2,1)S(1)} async-done(((bf16[32,4,128]{2,1,0:T(4,128)(2,1)}), bf16[32,4,128]{2,1,0:T(4,128)(2,1)S(1)}, u32[]{:S(2)}, u32[]{:S(2)}) %all-to-all-start) | async-done | bytes 32800 | tf_op jit(solution)/shard_map/all_to_all | solution.py:14
  101.8 0.2 convert_element_type.117
  101.9 0.1 fusion.15
  102.1 0.1 fusion
  102.3 22.6 %all_to_all.40 = bf16[16,4,513]{2,1,0:T(4,128)(2,1)S(1)} all-to-all(bf16[16,4,513]{2,1,0:T(4,128)(2,1)S(1)} %pad_maximum_fusion.1), channel_id=1, replica_groups=mesh['grp'=2,'tp'=16,'y'=16,'c'=2] {'y'}, dimensions={0} | all-to-all | bytes 131328 | tf_op jit(solution)/shard_map/all_to_all | solution.py:14
  125.0 0.1 fusion.46
  125.2 0.3 fusion.8
  125.5 0.1 multiply_reduce_fusion.1
  125.8 14.3 %all_to_all.41 = bf16[16,4,128]{2,1,0:T(4,128)(2,1)S(1)} all-to-all(bf16[16,4,128]{2,1,0:T(4,128)(2,1)S(1)} %broadcast_in_dim.24), channel_id=1, replica_groups=mesh['grp'=2,'tp'=16,'y'=16,'c'=2] {'y'}, dimensions={0} | all-to-all | bytes 32768 | tf_op jit(solution)/shard_map/all_to_all | solution.py:14
  140.1 0.1 convolution_convert_fusion.1
  140.2 0.1 convolution_convert_fusion
  140.4 7.8 %all_to_all.42 = bf16[4,16,256]{2,1,0:T(8,128)(2,1)S(1)} all-to-all(bf16[4,16,256]{2,1,0:T(8,128)(2,1)S(1)} %pad_maximum_fusion.3), channel_id=1, replica_groups={{0,32,64,96},{128,160,192,224},{256,288,320,352},{384,416,448,480},{1,3..., dimensions={0} | all-to-all | bytes 65536 | tf_op jit(solution)/shard_map/all_to_all | solution.py:14
  148.2 16.7 %all_to_all.43 = bf16[16,16,256]{2,1,0:T(8,128)(2,1)S(1)} all-to-all(bf16[16,16,256]{2,1,0:T(8,128)(2,1)S(1)} %broadcast_in_dim.25), channel_id=1, replica_groups=mesh['grp'=2,'tp'=16,'y'=16,'c'=2] {'tp'}, dimensions={0} | all-to-all | bytes 262144 | tf_op jit(solution)/shard_map/all_to_all | solution.py:14
  165.0 0.1 fusion.14
  165.1 0.1 fusion.1
  165.3 0.1 convert_element_type.118
  165.5 14.4 %all_to_all.44 = bf16[16,4,513]{2,1,0:T(4,128)(2,1)S(1)} all-to-all(bf16[16,4,513]{2,1,0:T(4,128)(2,1)S(1)} %pad_maximum_fusion.2), channel_id=1, replica_groups=mesh['grp'=2,'tp'=16,'y'=16,'c'=2] {'y'}, dimensions={0} | all-to-all | bytes 131328 | tf_op jit(solution)/shard_map/all_to_all | solution.py:14
  179.9 0.1 fusion.40
  180.1 0.3 fusion.5
  180.5 0.1 multiply_reduce_fusion
  180.7 14.5 %all_to_all.45 = bf16[16,4,128]{2,1,0:T(4,128)(2,1)S(1)} all-to-all(bf16[16,4,128]{2,1,0:T(4,128)(2,1)S(1)} %broadcast_in_dim.26), channel_id=1, replica_groups=mesh['grp'=2,'tp'=16,'y'=16,'c'=2] {'y'}, dimensions={0} | all-to-all | bytes 32768 | tf_op jit(solution)/shard_map/all_to_all | solution.py:14
  195.2 0.1 fusion.2
  195.3 0.1 broadcast_select_fusion.3
  195.6 23.1 %all_to_all.46 = bf16[32,4,128]{2,1,0:T(4,128)(2,1)S(1)} all-to-all(bf16[32,4,128]{2,1,0:T(4,128)(2,1)S(1)} %copy.85), channel_id=1, replica_groups=mesh['grp'=2,'tp'=16,'y'=16,'c'=2] {'tp','c'}, dimensions={0} | all-to-all | bytes 65536 | tf_op jit(solution)/shard_map/all_to_all | solution.py:14
  218.7 0.6 bitcast_reduce_fusion
  219.3 1.1 multiply_add_fusion
  (52 shorter events, 1.3 us)
Async XLA Ops:
  0.6 88.7 %copy-start.2 = (bf16[2,128,128]{2,1,0:T(8,128)(2,1)S(1)}, bf16[2,128,128]{2,1,0:T(8,128)(2,1)}, u32[]{:S(2)}) copy-start(bf16[2,128,128]{2,1,0:T(8,128)(2,1)} %param.15) | copy-start | bytes 196612
  2.0 87.4 %copy-start.3 = (f32[2,128]{1,0:T(2,128)S(1)}, f32[2,128]{1,0:T(2,128)}, u32[]{:S(2)}) copy-start(f32[2,128]{1,0:T(2,128)} %param.11) | copy-start | bytes 3076
  2.0 99.5 %all-to-all-start = ((bf16[32,4,128]{2,1,0:T(4,128)(2,1)}), bf16[32,4,128]{2,1,0:T(4,128)(2,1)S(1)}, u32[]{:S(2)}, u32[]{:S(2)}) async-start(bf16[32,4,128]{2,1,0:T(4,128)(2,1)} %bitcast.1), calls=%async_computation | async-start | bytes 65536 | tf_op jit(solution)/shard_map/all_to_all | solution.py:14
  89.3 1.1 copy-start.1
  90.5 11.6 %collective-permute-start = (bf16[2,128,640]{2,1,0:T(8,128)(2,1)S(1)}, bf16[2,128,640]{2,1,0:T(8,128)(2,1)S(1)}, u32[]{:S(2)}, u32[]{:S(2)}) collective-permute-start(bf16[2,128,640]{2,1,0:T(8,128)(2,1)S(1)} %pad_maximum_fusion), channel_id=1, source_target_pairs={{0,1},{1,0},{2,3},{3,2},{4,5},{5,4},{6,7},{7,6},{8,9},{9,8},{10,11... | collective-permute-start | bytes 983048 | tf_op jit(solution)/shard_map/ppermute | solution.py:42
  93.5 0.7 copy-start.4
  94.2 0.7 copy-start.5
  102.1 23.1 %copy-start = (f32[2,4,1,128,128]{4,3,2,1,0:T(8,128)S(1)}, f32[2,4,1,128,128]{4,3,2,1,0:T(8,128)}, u32[]{:S(2)}) copy-start(f32[2,4,1,128,128]{4,3,2,1,0:T(8,128)} %param.19) | copy-start | bytes 1572868

commit v5 on v4

--- a/solution.py
+++ b/solution.py
@@ -33,27 +33,30 @@
     )
     got = exchange(sent.reshape(tp_size * c_size, local_seqs, width), ("tp", "c"))
     got = got.reshape(tp_size, c_size, local_seqs, width)
-    own = jnp.where(core == 0, got[:, 0], got[:, 1]).reshape(held, width)
-    mate = jnp.where(core == 0, got[:, 1], got[:, 0]).reshape(held, width)
+    parts = [got[:, k].reshape(held, width) for k in range(c_size)]
 
     joined = jnp.concatenate([w_query, w_forget, w_value, w_gate], axis=2)
     joined = (joined.astype(F32) * norm_gain[:, :, None]).astype(BF16)
     packed = jnp.concatenate([joined, w_out], axis=2)
     other = lax.ppermute(packed, "c", [(0, 1), (1, 0)])
     proj_width = joined.shape[2]
+    ordered = [jnp.where(core == k, packed, other) for k in range(c_size)]
 
     mine = (lax.broadcasted_iota(jnp.int32, (held, width), 0) // local_seqs == tp).astype(F32)
     bounds = [jnp.broadcast_to(lower_bound[k], (local_seqs, lower_bound.shape[1])) for k in range(2)]
     gains = [jnp.broadcast_to(head_gain[k], (local_seqs, head_count, HD)) for k in range(2)]
-    own, mate, mine, bounds, gains = lax.optimization_barrier((own, mate, mine, bounds, gains))
+    ones = jnp.ones((width, width), BF16)
+    parts, mine, bounds, gains, ordered, ones = lax.optimization_barrier(
+        (parts, mine, bounds, gains, ordered, ones)
+    )
 
     steps = []
     for layer in range(2):
-        own_f, mate_f = own.astype(F32), mate.astype(F32)
-        squares = jnp.sum(own_f * own_f + mate_f * mate_f, axis=1, keepdims=True)
-        partial = dot(own, packed[layer, :, :proj_width]) + dot(mate, other[layer, :, :proj_width])
+        wide = [part.astype(F32) for part in parts]
+        squares = dot(sum(w * w for w in wide).astype(BF16), ones)
+        partial = sum(dot(p, w[layer, :, :proj_width]) for p, w in zip(parts, ordered))
         payload = jnp.concatenate([partial.astype(BF16), squares.astype(BF16)], axis=1)
-        got = exchange(payload.reshape(y_size, local_seqs, proj_width + 1), "y")
+        got = exchange(payload.reshape(y_size, local_seqs, proj_width + width), "y")
         total = jnp.sum(got.astype(F32), axis=0)
         factor = lax.rsqrt(total[:, proj_width:] / D + 1e-06)
         head_width = proj_width // 4
@@ -84,26 +87,26 @@
         )
         got = exchange(jnp.broadcast_to(normed[None], (y_size, *normed.shape)), "y")
         gathered = got.reshape(held, head_count * HD)
-        mixed_own = dot(gathered, packed[layer, :, proj_width:])
-        mixed_mate = dot(gathered, other[layer, :, proj_width:])
+        mixed = [dot(gathered, w[layer, :, proj_width:]) for w in ordered]
         if layer == 0:
             near = min(NEAR, tp_size)
             groups = [[j * near + i for i in range(near)] for j in range(tp_size // near)]
-            mixed = jnp.concatenate([mixed_own, mixed_mate], axis=1).astype(BF16)
+            mixed = jnp.concatenate(mixed, axis=1).astype(BF16)
             got = exchange(mixed.reshape(near, held // near, 2 * width), "tp", groups)
             piece = jnp.sum(got.astype(F32), axis=0).astype(BF16)
             got = exchange(jnp.broadcast_to(piece[None], (tp_size, *piece.shape)), "tp")
             got = got.reshape(tp_size // near, near, held // near, 2 * width)
             mixed = jnp.sum(got.astype(F32), axis=0).reshape(held, 2 * width)
-            own = (own_f + mixed[:, :width]).astype(BF16)
-            mate = (mate_f + mixed[:, width:]).astype(BF16)
+            parts = [
+                (w + mixed[:, k * width : (k + 1) * width]).astype(BF16) for k, w in enumerate(wide)
+            ]
         else:
-            mixed_own = (mixed_own + mine * own_f).astype(BF16)
-            mixed_mate = (mixed_mate + mine * mate_f).astype(BF16)
-            first = jnp.where(core == 0, mixed_own, mixed_mate)
-            second = jnp.where(core == 0, mixed_mate, mixed_own)
             sent = jnp.stack(
-                [a.reshape(tp_size, local_seqs, width) for a in (first, second)], axis=1
+                [
+                    (m + mine * w).astype(BF16).reshape(tp_size, local_seqs, width)
+                    for m, w in zip(mixed, wide)
+                ],
+                axis=1,
             )
             got = exchange(sent.reshape(tp_size * c_size, local_seqs, width), ("tp", "c"))
             got, steps = lax.optimization_barrier((got, steps))

time: 221 us -> 222 us (level)
  waiting for transfers between devices: 6.64 us -> 10.3 us
    all_to_all x1, starting transfers between devices: 87.3 us -> 4.17 us  [exchange(): return lax.all_to_all(x, axis, 0, 0, tiled=True, axis_index_groups=groups)]
    ppermute x1, starting transfers between devices: 2.97 us -> 85.4 us  [per_device(): other = lax.ppermute(packed, 'c', [(0, 1), (1, 0)])]
    all_to_all x1, waiting for transfers between devices: 6.64 us -> 10.3 us  [exchange(): return lax.all_to_all(x, axis, 0, 0, tiled=True, axis_index_groups=groups)]
  transfers between devices with their start and end apart: 2 -> 2, of which waited for: 1 -> 1; matrix products, arithmetic and copies ran while one was open for 1% -> 0% of each run, Pallas kernels for 0% -> 0%
where the time goes in v5:
time: 222 us
  blocking collectives  113 us (51%)
  starting transfers between devices  89.6 us (40%)
  waiting for transfers between devices  10.3 us (5%)
  other arithmetic  3.73 us (2%)
    all_to_all x7, blocking collectives, exchange(): return lax.all_to_all(x, axis, 0, 0, tiled=True, axis_index_groups=groups)  113 us
    ppermute x1, starting transfers between devices, per_device(): other = lax.ppermute(packed, 'c', [(0, 1), (1, 0)])  85.4 us
    all_to_all x1, waiting for transfers between devices, exchange(): return lax.all_to_all(x, axis, 0, 0, tiled=True, axis_index_groups=groups)  10.3 us
  transfers between devices with their start and end apart: 2, of which 1 were waited for; matrix products, arithmetic and copies ran while one was open for 0% of the time, Pallas kernels for 0%

profile of v5, /device:TPU:5, one launch (start us, length us, event | category | flops | bytes accessed | tf_op | source)
XLA Modules:
  0.0 221.8 jit_solution(13365898723396134907)
XLA Ops:
  0.6 1.1 multiply_convert_fusion
  1.8 85.4 %collective-permute-start = (bf16[2,128,640]{2,1,0:T(8,128)(2,1)S(1)}, bf16[2,128,640]{2,1,0:T(8,128)(2,1)S(1)}, u32[]{:S(2)}, u32[]{:S(2)}) collective-permute-start(bf16[2,128,640]{2,1,0:T(8,128)(2,1)S(1)} %pad_maximum_fusion), channel_id=1, source_target_pairs={{0,1},{1,0},{2,3},{3,2},{4,5},{5,4},{6,7},{7,6},{8,9},{9,8},{10,11... | collective-permute-start | bytes 983048 | tf_op jit(solution)/shard_map/ppermute | solution.py:41
  87.2 0.6 broadcast_in_dim.21
  87.8 4.2 %all-to-all-start = ((bf16[32,4,128]{2,1,0:T(4,128)(2,1)}), bf16[32,4,128]{2,1,0:T(4,128)(2,1)S(1)}, u32[]{:S(2)}, u32[]{:S(2)}) async-start(bf16[32,4,128]{2,1,0:T(4,128)(2,1)} %bitcast.1), calls=%async_computation | async-start | bytes 65536 | tf_op jit(solution)/shard_map/all_to_all | solution.py:14
  92.1 0.7 copy-done.3
  92.7 0.1 fusion.52
  92.8 0.6 copy-done.4
  93.4 10.3 %all-to-all-done = bf16[32,4,128]{2,1,0:T(4,128)(2,1)S(1)} async-done(((bf16[32,4,128]{2,1,0:T(4,128)(2,1)}), bf16[32,4,128]{2,1,0:T(4,128)(2,1)S(1)}, u32[]{:S(2)}, u32[]{:S(2)}) %all-to-all-start) | async-done | bytes 32800 | tf_op jit(solution)/shard_map/all_to_all | solution.py:14
  103.8 0.1 broadcast_select_fusion
  104.0 0.1 fusion.15
  104.2 0.1 convolution_convert_fusion.3
  104.3 0.1 fusion
  104.5 22.7 %all_to_all.40 = bf16[16,4,640]{2,1,0:T(4,128)(2,1)S(1)} all-to-all(bf16[16,4,640]{2,1,0:T(4,128)(2,1)S(1)} %reshape.154), channel_id=1, replica_groups=mesh['grp'=2,'tp'=16,'y'=16,'c'=2] {'y'}, dimensions={0} | all-to-all | bytes 163840 | tf_op jit(solution)/shard_map/all_to_all | solution.py:14
  127.3 0.3 fusion.6
  127.7 0.1 multiply_reduce_fusion.1
  127.9 14.4 %all_to_all.41 = bf16[16,4,128]{2,1,0:T(4,128)(2,1)S(1)} all-to-all(bf16[16,4,128]{2,1,0:T(4,128)(2,1)S(1)} %broadcast_in_dim.53), channel_id=1, replica_groups=mesh['grp'=2,'tp'=16,'y'=16,'c'=2] {'y'}, dimensions={0} | all-to-all | bytes 32768 | tf_op jit(solution)/shard_map/all_to_all | solution.py:14
  142.2 0.1 convolution_convert_fusion.2
  142.3 0.1 convolution_convert_fusion.1
  142.5 7.8 %all_to_all.42 = bf16[4,16,256]{2,1,0:T(8,128)(2,1)S(1)} all-to-all(bf16[4,16,256]{2,1,0:T(8,128)(2,1)S(1)} %pad_maximum_fusion.3), channel_id=1, replica_groups={{0,32,64,96},{128,160,192,224},{256,288,320,352},{384,416,448,480},{1,3..., dimensions={0} | all-to-all | bytes 65536 | tf_op jit(solution)/shard_map/all_to_all | solution.py:14
  150.3 15.9 %all_to_all.43 = bf16[16,16,256]{2,1,0:T(8,128)(2,1)S(1)} all-to-all(bf16[16,16,256]{2,1,0:T(8,128)(2,1)S(1)} %broadcast_in_dim.54), channel_id=1, replica_groups=mesh['grp'=2,'tp'=16,'y'=16,'c'=2] {'tp'}, dimensions={0} | all-to-all | bytes 262144 | tf_op jit(solution)/shard_map/all_to_all | solution.py:14
  166.2 0.1 fusion.13
  166.4 0.1 convolution_convert_fusion
  166.5 0.2 fusion.1
  166.7 14.4 %all_to_all.44 = bf16[16,4,640]{2,1,0:T(4,128)(2,1)S(1)} all-to-all(bf16[16,4,640]{2,1,0:T(4,128)(2,1)S(1)} %reshape.157), channel_id=1, replica_groups=mesh['grp'=2,'tp'=16,'y'=16,'c'=2] {'y'}, dimensions={0} | all-to-all | bytes 163840 | tf_op jit(solution)/shard_map/all_to_all | solution.py:14
  181.1 0.3 fusion.3
  181.5 0.1 multiply_reduce_fusion
  181.7 14.5 %all_to_all.45 = bf16[16,4,128]{2,1,0:T(4,128)(2,1)S(1)} all-to-all(bf16[16,4,128]{2,1,0:T(4,128)(2,1)S(1)} %broadcast_in_dim.55), channel_id=1, replica_groups=mesh['grp'=2,'tp'=16,'y'=16,'c'=2] {'y'}, dimensions={0} | all-to-all | bytes 32768 | tf_op jit(solution)/shard_map/all_to_all | solution.py:14
  196.2 0.1 fusion.35
  196.3 0.1 fusion.37
  196.6 23.5 %all_to_all.46 = bf16[32,4,128]{2,1,0:T(4,128)(2,1)S(1)} all-to-all(bf16[32,4,128]{2,1,0:T(4,128)(2,1)S(1)} %copy.38), channel_id=1, replica_groups=mesh['grp'=2,'tp'=16,'y'=16,'c'=2] {'tp','c'}, dimensions={0} | all-to-all | bytes 65536 | tf_op jit(solution)/shard_map/all_to_all | solution.py:14
  220.1 0.6 bitcast_reduce_fusion
  220.7 1.1 multiply_add_fusion
  (49 shorter events, 0.8 us)
Async XLA Ops:
  0.6 1.1 copy-start.1
  1.7 85.5 %copy-start.2 = (bf16[8,128]{1,0:T(8,128)(2,1)S(1)}, bf16[8,128]{1,0:T(8,128)(2,1)}, u32[]{:S(2)}) copy-start(bf16[8,128]{1,0:T(8,128)(2,1)} %param.10) | copy-start | bytes 6148
  1.8 102.0 %collective-permute-start = (bf16[2,128,640]{2,1,0:T(8,128)(2,1)S(1)}, bf16[2,128,640]{2,1,0:T(8,128)(2,1)S(1)}, u32[]{:S(2)}, u32[]{:S(2)}) collective-permute-start(bf16[2,128,640]{2,1,0:T(8,128)(2,1)S(1)} %pad_maximum_fusion), channel_id=1, source_target_pairs={{0,1},{1,0},{2,3},{3,2},{4,5},{5,4},{6,7},{7,6},{8,9},{9,8},{10,11... | collective-permute-start | bytes 983048 | tf_op jit(solution)/shard_map/ppermute | solution.py:41
  87.8 15.9 %all-to-all-start = ((bf16[32,4,128]{2,1,0:T(4,128)(2,1)}), bf16[32,4,128]{2,1,0:T(4,128)(2,1)S(1)}, u32[]{:S(2)}, u32[]{:S(2)}) async-start(bf16[32,4,128]{2,1,0:T(4,128)(2,1)} %bitcast.1), calls=%async_computation | async-start | bytes 65536 | tf_op jit(solution)/shard_map/all_to_all | solution.py:14
  92.1 0.7 copy-start.3
  92.7 0.7 copy-start.4
  104.2 23.2 %copy-start = (f32[2,4,1,128,128]{4,3,2,1,0:T(8,128)S(1)}, f32[2,4,1,128,128]{4,3,2,1,0:T(8,128)}, u32[]{:S(2)}) copy-start(f32[2,4,1,128,128]{4,3,2,1,0:T(8,128)} %param.19) | copy-start | bytes 1572868
